TPU v7x, 512 devices: a 8x2x16 block of a 8x8x16 slice. The times are simulated.
512 devices in a mesh: grp: 2 (over y), sp: 32 (over z, core), tp: 8 (over x).
Axes of the slice: x: 8, y: 2, z: 16, core: 2. Of those that a mesh axis runs over, the one named last changes fastest.
The devices are a block of a 8x8x16 slice.
Arguments:
- tokens_in: bfloat16 [16384, 2048], P(('grp', 'sp'), 'tp'), parts along dimension 0, may hold values from -6 to 6
- norm_gain: float32 [3, 2048], replicated, may hold values from 0.1 to 1.9
- w_pool_in: bfloat16 [3, 2048, 1024], P(None, 'sp', 'tp'), may hold values from -0.125 to 0.125
- w_gate: bfloat16 [3, 2048, 2048], P(None, 'sp', 'tp'), may hold values from -0.125 to 0.125
- w_back: bfloat16 [3, 1024, 2048], P(None, 'tp', 'sp'), may hold values from -0.375 to 0.375
Outputs:
- tokens_out: bfloat16 [16384, 2048], P(('grp', 'sp'), 'tp'), parts along dimension 0
There are 2 independent parts, one for each index of `grp`. A program takes and returns all parts, laid end to end along the dimension named above; an argument that names none is the same for every part. Nothing has to cross between parts.
All inputs are finite; a program needn't handle non-finite values.
Results may differ from a plain program's by a relative error of at most 0.017.
Values may be sent and summed in bfloat16 or wider, within the bound.
A program may use at most 64 MiB of HBM per device.

v0:
```python
import jax
import jax.numpy as jnp
from jax import lax
from jax.sharding import PartitionSpec as P

POOL_WIDTH = 1024
GROUPS = 4
GRID_W = 32
LAYERS = 3


pool_windows = (2, 4, 8, 16)
norm_eps = 1e-06


def rows_first(arrays, axis, dims):
    turned = [jnp.moveaxis(a, dim, 0) for a, dim in zip(arrays, dims)]
    both = jnp.concatenate([t.reshape(len(t), -1) for t in turned], axis=1)
    out, at, outs = (lax.all_gather(both, axis, axis=0, tiled=True), 0, [])
    for t, dim in zip(turned, dims):
        section = out[:, at : at + t[0].size].reshape(-1, *t.shape[1:])
        outs.append(jnp.moveaxis(section, 0, dim))
        at += t[0].size
    return tuple(outs)


def copy_for_each(value, axis):
    peers = lax.axis_size(axis)
    return lax.all_to_all(
        jnp.broadcast_to(value[None], (peers, *value.shape)), axis, 0, 0, tiled=True
    )


def laid_out(parts, dim):
    parts = jnp.moveaxis(parts, 0, dim)
    shape = parts.shape
    return parts.reshape(*shape[:dim], shape[dim] * shape[dim + 1], *shape[dim + 2 :])


def collect(value, axis, dim):
    parts = copy_for_each(value, axis)
    return laid_out(parts, dim)


def padded_2(value, sides, width):
    for axis, dim in sides:
        peers, length = (lax.axis_size(axis), value.shape[dim])
        up = [(i, (i + 1) % peers) for i in range(peers - 1)]
        down = [(j, i) for i, j in up]
        last = lax.slice_in_dim(value, length - width, length, axis=dim)
        initial = lax.slice_in_dim(value, 0, width, axis=dim)
        before = lax.ppermute(last, axis, up)
        after = lax.ppermute(initial, axis, down)
        value = jnp.concatenate([before, value, after], axis=dim)
    return value


def in_blocks(value, dim, peers):
    before, after = (value.shape[:dim], value.shape[dim + 1 :])
    return jnp.moveaxis(value.reshape(*before, peers, -1, *after), dim, 0)


def sum_at_owner(value, axis, dim):
    parts = in_blocks(value, dim, lax.axis_size(axis))
    arrived = lax.all_to_all(parts, axis, split_axis=0, concat_axis=0, tiled=True)
    return arrived.astype(jnp.float32).sum(axis=0)


def window_means(padded, rows_here, first_row, total_rows, window):
    reach = max(pool_windows) // 2
    half_span = window // 2
    width_cols = padded.shape[1] - 2 * reach
    row_sums = padded[reach - half_span : reach - half_span + rows_here]
    for offset in range(1 - half_span, half_span):
        row_sums = row_sums + padded[reach + offset : reach + offset + rows_here]
    box_sums = row_sums[:, reach - half_span : reach - half_span + width_cols]
    for offset in range(1 - half_span, half_span):
        box_sums = box_sums + row_sums[:, reach + offset : reach + offset + width_cols]
    row_index = first_row + jnp.arange(rows_here, dtype=jnp.int32)
    col_index = jnp.arange(width_cols, dtype=jnp.int32)
    row_counts = jnp.minimum(row_index + half_span, total_rows) - jnp.maximum(
        row_index - half_span, 0
    )
    col_counts = jnp.minimum(col_index + half_span, width_cols) - jnp.maximum(
        col_index - half_span, 0
    )
    counts = (row_counts[:, None] * col_counts[None, :]).astype(jnp.float32)
    return box_sums / counts[:, :, None]


def on_device(tokens_in, norm_gain, w_pool_in, w_gate, w_back):
    reach = max(pool_windows) // 2
    sp_count = lax.axis_size("sp")
    tp_pos = lax.axis_index("tp")
    sp_pos = lax.axis_index("sp")
    tok_rows = tokens_in.shape[0]
    rows_here = tok_rows // GRID_W
    total_rows = rows_here * sp_count
    first_row = sp_pos * rows_here
    local_pool = w_pool_in.shape[2]
    group_width = POOL_WIDTH // GROUPS
    channel_group = (tp_pos * local_pool + jnp.arange(local_pool, dtype=jnp.int32)) // group_width
    gathered = rows_first((w_pool_in, w_gate, w_back), "sp", (1, 1, 2))
    state = tokens_in
    for layer_id in range(LAYERS):
        whole_rows = collect(state, "tp", 1)
        wide = whole_rows.astype(jnp.float32)
        normed = (
            wide
            * lax.rsqrt(jnp.mean(wide * wide, axis=-1, keepdims=True) + norm_eps)
            * norm_gain[layer_id]
        ).astype(jnp.bfloat16)
        pool_acc = jnp.dot(normed, gathered[0][layer_id], preferred_element_type=jnp.float32)
        gate_acc = jnp.dot(normed, gathered[1][layer_id], preferred_element_type=jnp.float32)
        pool_in = pool_acc.astype(jnp.bfloat16)
        gate = jax.nn.sigmoid(gate_acc)
        cells = pool_in.reshape(rows_here, GRID_W, local_pool)
        rimmed = padded_2(cells, (("sp", 0),), reach)
        padded = jnp.pad(rimmed.astype(jnp.float32), ((0, 0), (reach, reach), (0, 0)))
        means = jnp.zeros((rows_here, GRID_W, local_pool), jnp.float32)
        for group_id in range(GROUPS):
            in_group = (channel_group == group_id)[None, None, :]
            means = jnp.where(
                in_group,
                window_means(padded, rows_here, first_row, total_rows, pool_windows[group_id]),
                means,
            )
        pooled = (
            (means - cells.astype(jnp.float32)).reshape(tok_rows, local_pool).astype(jnp.bfloat16)
        )
        terms = jnp.dot(pooled, gathered[2][layer_id], preferred_element_type=jnp.float32)
        branch = sum_at_owner(terms.astype(jnp.bfloat16), "tp", 1)
        state = (state.astype(jnp.float32) + gate * branch).astype(jnp.bfloat16)
    return state


def solution(mesh):
    return jax.shard_map(
        on_device,
        mesh=mesh,
        in_specs=(
            P(("grp", "sp"), "tp"),
            P(),
            P(None, "sp", "tp"),
            P(None, "sp", "tp"),
            P(None, "tp", "sp"),
        ),
        out_specs=P(("grp", "sp"), "tp"),
        check_vma=False,
    )
```

profile of v0, /device:TPU:65, one launch (start us, length us, event | category | flops | bytes accessed | tf_op | source)
XLA Modules:
  0.0 339.2 jit_solution(322811398811000513)
XLA Ops:
  6.6 0.9 copy.43
  7.5 0.8 copy_bitcast_fusion
  8.3 0.7 pad_maximum_fusion
  9.1 1.0 copy.21
  10.1 1.1 broadcast_in_dim.53
  11.1 7.9 %all-to-all-start = ((bf16[8,256,256]{1,2,0:T(8,128)(2,1)}), bf16[8,256,256]{1,2,0:T(8,128)(2,1)S(1)}, u32[]{:S(2)}, u32[]{:S(2)}) async-start(bf16[8,256,256]{1,2,0:T(8,128)(2,1)} %broadcast_in_dim.53), calls=%async_computation | async-start | bytes 2097152 | tf_op jit(solution)/shard_map/all_to_all | solution.py:29
  19.5 17.3 %all-to-all-done = bf16[8,256,256]{1,2,0:T(8,128)(2,1)S(1)} async-done(((bf16[8,256,256]{1,2,0:T(8,128)(2,1)}), bf16[8,256,256]{1,2,0:T(8,128)(2,1)S(1)}, u32[]{:S(2)}, u32[]{:S(2)}) %all-to-all-start) | async-done | bytes 1048608 | tf_op jit(solution)/shard_map/all_to_all | solution.py:29
  37.1 1.3 fusion.2
  38.4 84.4 %all-gather.2.cloned.1.call-done = bf16[2048,1536]{1,0:T(8,128)(2,1)} async-done(((bf16[64,1536]{1,0:T(8,128)(2,1)}), bf16[2048,1536]{1,0:T(8,128)(2,1)}) %all-gather.2.cloned.1.call-update) | async-done | bytes 6291472 | tf_op jit(solution)/shard_map/all_gather | solution.py:19
  122.8 2.2 fusion.97
  125.1 1.7 copy.27
  126.7 1.8 convolution_convert_fusion.5
  128.6 2.2 collective-permute-start.1
  130.8 3.4 %collective-permute-start = (bf16[8,32,128]{2,1,0:T(8,128)(2,1)S(1)}, bf16[8,32,128]{2,1,0:T(8,128)(2,1)S(1)}, u32[]{:S(2)}, u32[]{:S(2)}) collective-permute-start(bf16[8,32,128]{2,1,0:T(8,128)(2,1)S(1)} %bitcast.124), channel_id=1, source_target_pairs={{0,8},{8,16},{16,24},{24,32},{32,40},{40,48},{48,56},{56,64},{64,7... | collective-permute-start | bytes 196616 | tf_op jit(solution)/shard_map/ppermute | solution.py:52
  134.2 0.8 copy.29
  135.0 0.5 collective-permute-done
  135.8 0.4 fusion.82
  136.3 0.4 convolution_convert_fusion.2
  136.7 1.1 copy.52
  137.8 6.6 %all-to-all-start.1 = ((bf16[8,256,256]{2,1,0:T(8,128)(2,1)}), bf16[8,256,256]{2,1,0:T(8,128)(2,1)}, u32[]{:S(2)}, u32[]{:S(2)}) async-start(bf16[8,256,256]{2,1,0:T(8,128)(2,1)} %bitcast.101), calls=%async_computation.1 | async-start | bytes 2097152 | tf_op jit(solution)/shard_map/all_to_all | solution.py:65
  144.3 1.9 slice-done
  146.2 3.0 copy.25
  149.2 24.4 %all-to-all-done.1 = bf16[8,256,256]{2,1,0:T(8,128)(2,1)} async-done(((bf16[8,256,256]{2,1,0:T(8,128)(2,1)}), bf16[8,256,256]{2,1,0:T(8,128)(2,1)}, u32[]{:S(2)}, u32[]{:S(2)}) %all-to-all-start.1) | async-done | bytes 1048608 | tf_op jit(solution)/shard_map/all_to_all | solution.py:65
  173.6 1.4 convert_reduce_fusion.2
  175.0 2.0 fusion.24
  177.1 1.1 broadcast_in_dim.58
  178.2 3.8 %all-to-all-start.2 = ((bf16[8,256,256]{1,2,0:T(8,128)(2,1)}), bf16[8,256,256]{1,2,0:T(8,128)(2,1)S(1)}, u32[]{:S(2)}, u32[]{:S(2)}) async-start(bf16[8,256,256]{1,2,0:T(8,128)(2,1)} %broadcast_in_dim.58), calls=%async_computation.2 | async-start | bytes 2097152 | tf_op jit(solution)/shard_map/all_to_all | solution.py:29
  182.0 26.8 %all-to-all-done.2 = bf16[8,256,256]{1,2,0:T(8,128)(2,1)S(1)} async-done(((bf16[8,256,256]{1,2,0:T(8,128)(2,1)}), bf16[8,256,256]{1,2,0:T(8,128)(2,1)S(1)}, u32[]{:S(2)}, u32[]{:S(2)}) %all-to-all-start.2) | async-done | bytes 1048608 | tf_op jit(solution)/shard_map/all_to_all | solution.py:29
  209.4 1.5 convolution_convert_fusion.4
  210.9 4.7 %collective-permute-start.3 = (bf16[8,32,128]{2,1,0:T(8,128)(2,1)S(1)}, bf16[8,32,128]{2,1,0:T(8,128)(2,1)S(1)}, u32[]{:S(2)}, u32[]{:S(2)}) collective-permute-start(bf16[8,32,128]{2,1,0:T(8,128)(2,1)S(1)} %bitcast.131), channel_id=1, source_target_pairs={{8,0},{16,8},{24,16},{32,24},{40,32},{48,40},{56,48},{64,56},{72,6... | collective-permute-start | bytes 196616 | tf_op jit(solution)/shard_map/ppermute | solution.py:53
  215.6 2.9 collective-permute-start.2
  218.5 1.3 collective-permute-done.2
  220.1 0.4 fusion.83
  220.5 1.0 copy-done.2
  221.5 0.4 convolution_convert_fusion.1
  222.0 31.2 %all_to_all.30 = bf16[8,256,256]{2,1,0:T(8,128)(2,1)S(1)} all-to-all(bf16[8,256,256]{2,1,0:T(8,128)(2,1)S(1)} %bitcast.108), channel_id=1, replica_groups=mesh['grp'=2,'sp'=32,'tp'=8] {'tp'}, dimensions={0} | all-to-all | bytes 2097152 | tf_op jit(solution)/shard_map/all_to_all | solution.py:65
  253.3 1.8 fusion.25
  255.2 1.1 broadcast_in_dim.59
  256.3 3.8 %all-to-all-start.4 = ((bf16[8,256,256]{1,2,0:T(8,128)(2,1)}), bf16[8,256,256]{1,2,0:T(8,128)(2,1)S(1)}, u32[]{:S(2)}, u32[]{:S(2)}) async-start(bf16[8,256,256]{1,2,0:T(8,128)(2,1)} %broadcast_in_dim.59), calls=%async_computation.4 | async-start | bytes 2097152 | tf_op jit(solution)/shard_map/all_to_all | solution.py:29
  260.0 26.8 %all-to-all-done.4 = bf16[8,256,256]{1,2,0:T(8,128)(2,1)S(1)} async-done(((bf16[8,256,256]{1,2,0:T(8,128)(2,1)}), bf16[8,256,256]{1,2,0:T(8,128)(2,1)S(1)}, u32[]{:S(2)}, u32[]{:S(2)}) %all-to-all-start.4) | async-done | bytes 1048608 | tf_op jit(solution)/shard_map/all_to_all | solution.py:29
  287.5 1.5 convolution_convert_fusion.3
  289.0 4.7 %collective-permute-start.5 = (bf16[8,32,128]{2,1,0:T(8,128)(2,1)S(1)}, bf16[8,32,128]{2,1,0:T(8,128)(2,1)S(1)}, u32[]{:S(2)}, u32[]{:S(2)}) collective-permute-start(bf16[8,32,128]{2,1,0:T(8,128)(2,1)S(1)} %bitcast.127), channel_id=1, source_target_pairs={{8,0},{16,8},{24,16},{32,24},{40,32},{48,40},{56,48},{64,56},{72,6... | collective-permute-start | bytes 196616 | tf_op jit(solution)/shard_map/ppermute | solution.py:53
  293.7 2.0 collective-permute-start.4
  295.7 1.3 collective-permute-done.4
  297.2 0.4 fusion.84
  297.6 0.4 convolution_convert_fusion
  298.1 31.6 %all_to_all.31 = bf16[8,256,256]{2,1,0:T(8,128)(2,1)S(1)} all-to-all(bf16[8,256,256]{2,1,0:T(8,128)(2,1)S(1)} %bitcast.109), channel_id=1, replica_groups=mesh['grp'=2,'sp'=32,'tp'=8] {'tp'}, dimensions={0} | all-to-all | bytes 2097152 | tf_op jit(solution)/shard_map/all_to_all | solution.py:65
  329.9 2.4 fusion.26
  (54 shorter events, 3.5 us)
Async XLA Ops:
  6.5 0.9 copy-start
  6.6 116.3 %all-gather.2.cloned.1.call-start = ((), (), s32[]{:S(2)}) async-start(), calls=%async_computation.6 | async-start | bytes 6488064 | tf_op jit(solution)/shard_map/all_gather | solution.py:19
  8.3 10.7 %copy-start.4 = (f32[3,2048]{1,0:T(4,128)S(1)}, f32[3,2048]{1,0:T(4,128)}, u32[]{:S(2)}) copy-start(f32[3,2048]{1,0:T(4,128)} %param.6) | copy-start | bytes 73732
  11.1 25.7 %all-to-all-start = ((bf16[8,256,256]{1,2,0:T(8,128)(2,1)}), bf16[8,256,256]{1,2,0:T(8,128)(2,1)S(1)}, u32[]{:S(2)}, u32[]{:S(2)}) async-start(bf16[8,256,256]{1,2,0:T(8,128)(2,1)} %broadcast_in_dim.53), calls=%async_computation | async-start | bytes 2097152 | tf_op jit(solution)/shard_map/all_to_all | solution.py:29
  128.6 6.4 %collective-permute-start.1 = (bf16[8,32,128]{2,1,0:T(8,128)(2,1)S(1)}, bf16[8,32,128]{2,1,0:T(8,128)(2,1)S(1)}, u32[]{:S(2)}, u32[]{:S(2)}) collective-permute-start(bf16[8,32,128]{2,1,0:T(8,128)(2,1)S(1)} %bitcast.123), channel_id=1, source_target_pairs={{8,0},{16,8},{24,16},{32,24},{40,32},{48,40},{56,48},{64,56},{72,6... | collective-permute-start | bytes 196616 | tf_op jit(solution)/shard_map/ppermute | solution.py:53
  130.8 4.7 %collective-permute-start = (bf16[8,32,128]{2,1,0:T(8,128)(2,1)S(1)}, bf16[8,32,128]{2,1,0:T(8,128)(2,1)S(1)}, u32[]{:S(2)}, u32[]{:S(2)}) collective-permute-start(bf16[8,32,128]{2,1,0:T(8,128)(2,1)S(1)} %bitcast.124), channel_id=1, source_target_pairs={{0,8},{8,16},{16,24},{24,32},{32,40},{40,48},{48,56},{56,64},{64,7... | collective-permute-start | bytes 196616 | tf_op jit(solution)/shard_map/ppermute | solution.py:52
  135.0 1.2 copy-start.1
  137.8 35.8 %all-to-all-start.1 = ((bf16[8,256,256]{2,1,0:T(8,128)(2,1)}), bf16[8,256,256]{2,1,0:T(8,128)(2,1)}, u32[]{:S(2)}, u32[]{:S(2)}) async-start(bf16[8,256,256]{2,1,0:T(8,128)(2,1)} %bitcast.101), calls=%async_computation.1 | async-start | bytes 2097152 | tf_op jit(solution)/shard_map/all_to_all | solution.py:65
  144.3 1.9 slice-start
  146.2 28.7 %copy-start.3 = (bf16[256,256]{1,0:T(8,128)(2,1)S(1)}, bf16[256,256]{1,0:T(8,128)(2,1)}, u32[]{:S(2)}) copy-start(bf16[256,256]{1,0:T(8,128)(2,1)} %param.5) | copy-start | bytes 393220
  178.2 30.5 %all-to-all-start.2 = ((bf16[8,256,256]{1,2,0:T(8,128)(2,1)}), bf16[8,256,256]{1,2,0:T(8,128)(2,1)S(1)}, u32[]{:S(2)}, u32[]{:S(2)}) async-start(bf16[8,256,256]{1,2,0:T(8,128)(2,1)} %broadcast_in_dim.58), calls=%async_computation.2 | async-start | bytes 2097152 | tf_op jit(solution)/shard_map/all_to_all | solution.py:29
  210.9 7.6 %collective-permute-start.3 = (bf16[8,32,128]{2,1,0:T(8,128)(2,1)S(1)}, bf16[8,32,128]{2,1,0:T(8,128)(2,1)S(1)}, u32[]{:S(2)}, u32[]{:S(2)}) collective-permute-start(bf16[8,32,128]{2,1,0:T(8,128)(2,1)S(1)} %bitcast.131), channel_id=1, source_target_pairs={{8,0},{16,8},{24,16},{32,24},{40,32},{48,40},{56,48},{64,56},{72,6... | collective-permute-start | bytes 196616 | tf_op jit(solution)/shard_map/ppermute | solution.py:53
  215.6 4.2 %collective-permute-start.2 = (bf16[8,32,128]{2,1,0:T(8,128)(2,1)S(1)}, bf16[8,32,128]{2,1,0:T(8,128)(2,1)S(1)}, u32[]{:S(2)}, u32[]{:S(2)}) collective-permute-start(bf16[8,32,128]{2,1,0:T(8,128)(2,1)S(1)} %bitcast.132), channel_id=1, source_target_pairs={{0,8},{8,16},{16,24},{24,32},{32,40},{40,48},{48,56},{56,64},{64,7... | collective-permute-start | bytes 196616 | tf_op jit(solution)/shard_map/ppermute | solution.py:52
  220.1 1.4 copy-start.2
  256.3 30.5 %all-to-all-start.4 = ((bf16[8,256,256]{1,2,0:T(8,128)(2,1)}), bf16[8,256,256]{1,2,0:T(8,128)(2,1)S(1)}, u32[]{:S(2)}, u32[]{:S(2)}) async-start(bf16[8,256,256]{1,2,0:T(8,128)(2,1)} %broadcast_in_dim.59), calls=%async_computation.4 | async-start | bytes 2097152 | tf_op jit(solution)/shard_map/all_to_all | solution.py:29
  289.0 6.6 %collective-permute-start.5 = (bf16[8,32,128]{2,1,0:T(8,128)(2,1)S(1)}, bf16[8,32,128]{2,1,0:T(8,128)(2,1)S(1)}, u32[]{:S(2)}, u32[]{:S(2)}) collective-permute-start(bf16[8,32,128]{2,1,0:T(8,128)(2,1)S(1)} %bitcast.127), channel_id=1, source_target_pairs={{8,0},{16,8},{24,16},{32,24},{40,32},{48,40},{56,48},{64,56},{72,6... | collective-permute-start | bytes 196616 | tf_op jit(solution)/shard_map/ppermute | solution.py:53
  293.7 3.3 collective-permute-start.4
Sparse Core Ops, SparseCore 0:
  9.5 113.3 all-gather.1
where the time goes:
time: 340 us; the launch traced here: 339 us
  waiting for transfers between devices  183 us (54%)
  blocking collectives  62.9 us (18%)
  starting transfers between devices  41.8 us (12%)
  local copies, waits for them, and re-layouts  18 us (5%)
  between operations  13.8 us (4%)
  matrix products  12.4 us (4%)
  other arithmetic  7.52 us (2%)
    all_gather x1, waiting for transfers between devices, rows_first(): out, at, outs = (lax.all_gather(both, axis, axis=0, tiled=True), 0, [])  84.4 us
    all_to_all x3, waiting for transfers between devices, copy_for_each(): lax.all_to_all(jnp.broadcast_to(value[None], (peers, *value.shape)), axis...  70.9 us
    all_to_all x2, blocking collectives, sum_at_owner(): lax.all_to_all(parts, axis, split_axis=0, concat_axis=0, tiled=True)  62.9 us
    all_to_all x1, waiting for transfers between devices, sum_at_owner(): lax.all_to_all(parts, axis, split_axis=0, concat_axis=0, tiled=True)  24.4 us
    all_to_all x3, starting transfers between devices, copy_for_each(): lax.all_to_all(jnp.broadcast_to(value[None], (peers, *value.shape)), axis...  15.4 us
    ppermute x3, starting transfers between devices, padded_2(): after = lax.ppermute(initial, axis, down)  11.6 us
    slice x6, local copies, waits for them, and re-layouts, rows_first(): section = out[:, at:at + t[0].size].reshape(-1, *t.shape[1:])  9.49 us
    ppermute x3, starting transfers between devices, padded_2(): before = lax.ppermute(last, axis, up)  8.25 us
  transfers between devices with their start and end apart: 11, of which 8 were waited for; matrix products, arithmetic and copies ran while one was open for 2% of the time, Pallas kernels for 0%

commit v1 on v0

v1 whole, which is shorter than its diff:
```python
import functools

import jax
import jax.numpy as jnp
from jax import lax
from jax.experimental import pallas as pl
from jax.experimental.pallas import tpu as pltpu
from jax.sharding import PartitionSpec as P

MESH = pl.DeviceIdType.MESH
F32 = jnp.float32
BF16 = jnp.bfloat16
GRID_W = 32
GROUPS = 4
EPS = 1e-6
CHUNKS = 2


def mixer(n_sp, n_tp, tok_ref, gain_ref, wpool_ref, wgate_ref, wback_ref, out_ref,
          xs, ps, xg, w_pg, w_b, pin, halo, boxm, inv_count, gate, sumsq, swap_src,
          x_recv, p_recv, a_recv, b_recv, halo_recv, peer_recv, swap_recv,
          x_send, p_send, a_send, b_send, peer_send, halo_send, swap_send):
    layers = gain_ref.shape[0]
    tokens, feat = tok_ref.shape
    chan = wpool_ref.shape[2]
    rows_w = wpool_ref.shape[1]
    ct = tokens // CHUNKS
    half_tp = n_tp // 2
    n_z = n_sp // 2
    half_z = n_z // 2
    q_n = n_sp // n_tp
    sp = lax.axis_index("sp")
    tp = lax.axis_index("tp")

    def tp_at(d):
        return lax.rem(tp + (d + n_tp), n_tp)

    def sp_at(d):
        return lax.rem(sp + (2 * d + n_sp), n_sp)

    peer = sp + 1 - 2 * lax.rem(sp, 2)
    before = lax.rem(sp + n_sp - 1, n_sp)
    after = lax.rem(sp + 1, n_sp)
    quad = lax.rem(sp, q_n)
    swap_to = (q_n * lax.rem(tp + half_tp, n_tp) + quad, sp // q_n)
    swap_from = (q_n * tp + quad, lax.rem(sp // q_n + half_tp, n_tp))

    barrier = pltpu.get_barrier_semaphore()
    greet = [{"tp": tp_at(1)}, {"tp": tp_at(-1)}, {"sp": before}, {"sp": after},
             {"sp": sp_at(1)}, {"sp": sp_at(-1)}, {"sp": sp_at(2)}, {"sp": sp_at(-2)},
             {"sp": swap_from[0], "tp": swap_from[1]}]
    for who in greet:
        pl.semaphore_signal(barrier, inc=1, device_id=who, device_id_type=MESH)

    own_rows = pl.ds(pl.multiple_of(sp * rows_w, rows_w), rows_w)
    for l in range(layers):
        w_pg[l, own_rows, 0:chan] = wpool_ref[l]
        w_pg[l, own_rows, chan:] = wgate_ref[l]
        swap_src[l] = wback_ref[l].astype(F32).T.astype(BF16)
    for c in range(CHUNKS):
        xs[0, c, tp] = tok_ref[c * ct:(c + 1) * ct, :]

    pl.semaphore_wait(barrier, len(greet))

    def start(src, dst, send, recv, who):
        pltpu.make_async_remote_copy(src_ref=src, dst_ref=dst, send_sem=send, recv_sem=recv,
                                     device_id=who, device_id_type=MESH).start()

    def arrived(ref, sem):
        pltpu.make_async_copy(ref, ref, sem).wait()

    def reach(way, c):
        if half_tp * 2 == n_tp and (c % 2 == 0) != (way == 0):
            return half_tp - 1
        return half_tp

    def x_start(buf, l, c, d, send, recv):
        for way in (0, 1):
            if d <= reach(way, c):
                x_start_way(buf, l, c, d, send, recv, way)

    def x_start_way(buf, l, c, d, send, recv, way):
        step = 1 if way == 0 else -1
        block = buf.at[l, c, tp_at(-step * (d - 1))]
        start(block, block, send.at[l], recv.at[l, way, d - 1, c], {"tp": tp_at(step)})

    def x_wait_way(buf, l, c, d, recv, way):
        step = 1 if way == 0 else -1
        arrived(buf.at[l, c, tp_at(-step * d)], recv.at[l, way, d - 1, c])

    def z_reach(way):
        return half_z if way == 0 else n_z - 1 - half_z

    def z_rows(d):
        return pl.ds(pl.multiple_of(sp_at(d) * rows_w, rows_w), rows_w)

    def z_send(buf, l, kind, d0, width, send, recv, way):
        step = 1 if way == 0 else -1
        piece = buf.at[l, z_rows(-step * d0)]
        for r in range(1, width + 1):
            if d0 + r <= z_reach(way):
                start(piece, piece, send.at[l], recv.at[l, way, d0 + r - 1], {"sp": sp_at(step * r)})

    def z_peer(buf, l, kind, d):
        piece = buf.at[l, z_rows(d)]
        start(piece, piece, peer_send.at[kind, l], peer_recv.at[kind, l], {"sp": peer})

    def z_begin(kind, l, width):
        buf, send, recv = z_parts(kind)
        for way in (0, 1):
            z_send(buf, l, kind, 0, width, send, recv, way)
        z_peer(buf, l, kind, 0)

    def z_parts(kind):
        return (w_pg, a_send, a_recv) if kind == 0 else (w_b, b_send, b_recv)

    def z_stage(kind, l, stage, width):
        buf, send, recv = z_parts(kind)
        for r in range(width, 0, -1):
            d = (stage - 1) * width + r
            for way in (0, 1):
                step = 1 if way == 0 else -1
                if d <= z_reach(way):
                    arrived(buf.at[l, z_rows(-step * d)], recv.at[l, way, d - 1])
                    if r == width:
                        z_send(buf, l, kind, d, width, send, recv, way)
                    z_peer(buf, l, kind, -step * d)

    def z_peers_done(kind, l):
        buf = z_parts(kind)[0]
        arrived(buf.at[l, pl.ds(0, n_z * rows_w)], peer_recv.at[kind, l])

    def prep(l, c, j):
        block = xs[l, c, j].astype(F32)
        lanes = pl.ds(pl.multiple_of(j * feat, feat), feat)
        squares = block * block
        part = squares[:, 0:128]
        for k in range(1, feat // 128):
            part = part + squares[:, k * 128:(k + 1) * 128]
        sumsq[c * ct:(c + 1) * ct, :] += part
        xg[c * ct:(c + 1) * ct, lanes] = (block * gain_ref[l, :, lanes]).astype(BF16)

    for c in range(CHUNKS):
        x_start(xs, 0, c, 1, x_send, x_recv)
        if c == 0:
            z_begin(0, 0, 2)
            start(swap_src, w_b.at[:, pl.ds(pl.multiple_of(swap_to[0] * rows_w, rows_w), rows_w)], swap_send, swap_recv,
                  {"sp": swap_to[0], "tp": swap_to[1]})

    window = lax.shift_left(2, (tp * chan) // (n_tp * chan // GROUPS))
    reach_w = window // 2
    grid_rows = tokens // GRID_W
    first = sp * grid_rows
    total = grid_rows * n_sp
    ti = lax.broadcasted_iota(jnp.int32, (tokens, tokens), 0)
    tj = lax.broadcasted_iota(jnp.int32, (tokens, tokens), 1)
    ri, ci = ti // GRID_W, ti % GRID_W
    cj = tj % GRID_W
    col_in = (cj >= ci - reach_w) & (cj < ci + reach_w)
    for k in range(3):
        rj = tj // GRID_W + (k - 1) * grid_rows
        inside = col_in & (rj >= ri - reach_w) & (rj < ri + reach_w)
        boxm[k] = jnp.where(inside, 1.0, 0.0).astype(BF16)
    tr = lax.broadcasted_iota(jnp.int32, (tokens, chan), 0)
    r_at, c_at = tr // GRID_W + first, tr % GRID_W
    r_n = jnp.minimum(r_at + reach_w, total) - jnp.maximum(r_at - reach_w, 0)
    c_n = jnp.minimum(c_at + reach_w, GRID_W) - jnp.maximum(c_at - reach_w, 0)
    inv_count[...] = 1.0 / (r_n * c_n).astype(F32)

    @pl.when(sp == 0)
    def _():
        for l in range(layers):
            halo[l, 0] = jnp.zeros((tokens, chan), BF16)

    @pl.when(sp == n_sp - 1)
    def _():
        for l in range(layers):
            halo[l, 1] = jnp.zeros((tokens, chan), BF16)

    for l in range(layers):
        sumsq[...] = jnp.zeros_like(sumsq)
        for c in range(CHUNKS):
            prep(l, c, tp)
        if l > 0:
            z_begin(1, l, 1)
        if l + 1 < layers and l > 0:
            z_begin(0, l + 1, 1)
        for d in range(1, half_tp + 1):
            for c in range(CHUNKS):
                for way in (0, 1):
                    if d <= reach(way, c):
                        x_wait_way(xs, l, c, d, x_recv, way)
                        if d + 1 <= reach(way, c):
                            x_start_way(xs, l, c, d + 1, x_send, x_recv, way)
                for way in (0, 1):
                    if d <= reach(way, c):
                        prep(l, c, tp_at(-d if way == 0 else d))
            if l == 0:
                z_stage(0, 0, d, 2)
            else:
                z_stage(0, l, half_tp + d, 1)
                z_stage(1, l, d, 1)
        z_peers_done(0, l)

        scale = lax.rsqrt(jnp.sum(sumsq[...], axis=1, keepdims=True) * (1.0 / (n_tp * feat)) + EPS)
        pool = jnp.dot(xg[...], w_pg[l, :, 0:chan], preferred_element_type=F32)
        pin[l] = (pool * scale).astype(BF16)

        @pl.when(sp > 0)
        def _():
            start(pin.at[l], halo.at[l, 1], halo_send.at[l, 1], halo_recv.at[l, 1], {"sp": before})

        @pl.when(sp < n_sp - 1)
        def _():
            start(pin.at[l], halo.at[l, 0], halo_send.at[l, 0], halo_recv.at[l, 0], {"sp": after})

        if l == 0:
            arrived(w_b.at[:, own_rows], swap_recv)
            z_begin(1, 0, 2)
        if l + 1 < layers and l == 0:
            z_begin(0, l + 1, 1)
        gate_acc = jnp.dot(xg[...], w_pg[l, :, chan:], preferred_element_type=F32)
        gate[...] = jax.nn.sigmoid(gate_acc * scale)
        own_pool = pin[l]
        box = jnp.dot(boxm[1], own_pool, preferred_element_type=F32)

        @pl.when(sp > 0)
        def _():
            arrived(halo.at[l, 0], halo_recv.at[l, 0])

        @pl.when(sp < n_sp - 1)
        def _():
            arrived(halo.at[l, 1], halo_recv.at[l, 1])

        box = box + jnp.dot(boxm[0], halo[l, 0], preferred_element_type=F32)
        box = box + jnp.dot(boxm[2], halo[l, 1], preferred_element_type=F32)
        pooled = (box * inv_count[...] - own_pool.astype(F32)).astype(BF16)
        for c in range(CHUNKS):
            ps[l, c, tp] = pooled[c * ct:(c + 1) * ct]
            x_start(ps, l, c, 1, p_send, p_recv)

        def finish(c):
            branch = None
            for p in range(n_tp):
                term = lax.dot_general(ps[l, c, (p + half_tp) % n_tp], w_b[l, p * feat:(p + 1) * feat],
                                       (((1,), (1,)), ((), ())), preferred_element_type=F32)
                branch = term if branch is None else branch + term
            rows = slice(c * ct, (c + 1) * ct)
            new = (xs[l, c, tp].astype(F32) + gate[rows] * branch).astype(BF16)
            if l + 1 < layers:
                xs[l + 1, c, tp] = new
                x_start(xs, l + 1, c, 1, x_send, x_recv)
            else:
                out_ref[rows, :] = new

        for d in range(1, half_tp + 1):
            if d == half_tp:
                if l == 0:
                    z_stage(1, 0, d, 2)
                else:
                    z_stage(1, l, half_tp + d, 1)
                if l + 1 < layers:
                    z_stage(0, l + 1, d, 1)
                z_peers_done(1, l)
            for c in range(CHUNKS):
                for way in (0, 1):
                    if d <= reach(way, c):
                        x_wait_way(ps, l, c, d, p_recv, way)
                        if d + 1 <= reach(way, c):
                            x_start_way(ps, l, c, d + 1, p_send, p_recv, way)
                if d == half_tp:
                    finish(c)
            if d < half_tp:
                if l == 0:
                    z_stage(1, 0, d, 2)
                else:
                    z_stage(1, l, half_tp + d, 1)
                if l + 1 < layers:
                    z_stage(0, l + 1, d, 1)

    x_sends = sum(reach(way, c) for way in (0, 1) for c in range(CHUNKS))
    z_sends = {}
    for width in (1, 2):
        z_sends[width] = sum(
            1 for way in (0, 1) for d0 in range(0, half_z, width) for r in range(1, width + 1)
            if d0 + r <= z_reach(way))
    arrived(swap_src, swap_send)

    def drained(sem, ref, count, size):
        while count:
            now = min(count, size)
            arrived(ref.at[pl.ds(0, now * (ref.shape[0] // size))], sem)
            count -= now

    for l in range(layers):
        for buf, send in ((xs, x_send), (ps, p_send)):
            arrived_many(buf, l, x_sends, send.at[l])
        for kind in (0, 1):
            buf, send, _ = z_parts(kind)
            width = 2 if l == 0 else 1
            drained(send.at[l], buf.at[l], z_sends[width], n_sp)
            drained(peer_send.at[kind, l], buf.at[l], n_z, n_sp)

        @pl.when(sp > 0)
        def _():
            arrived(pin.at[l], halo_send.at[l, 1])

        @pl.when(sp < n_sp - 1)
        def _():
            arrived(pin.at[l], halo_send.at[l, 0])


def arrived_many(buf, l, count, sem):
    per = buf.shape[2]
    c = 0
    while count:
        now = min(count, per)
        ref = buf.at[l, c % CHUNKS, pl.ds(0, now)]
        pltpu.make_async_copy(ref, ref, sem).wait()
        count -= now
        c += 1


def solution(mesh):
    n_sp, n_tp = mesh.shape["sp"], mesh.shape["tp"]

    def on_device(tokens_in, norm_gain, w_pool_in, w_gate, w_back):
        layers = norm_gain.shape[0]
        tokens, feat = tokens_in.shape
        rows_w, chan = w_pool_in.shape[1:]
        rows = n_sp * rows_w
        ct = tokens // CHUNKS
        half_tp = n_tp // 2
        half_z = n_sp // 4
        dma = pltpu.SemaphoreType.DMA
        vmem = pl.BlockSpec(memory_space=pltpu.VMEM)
        return pl.pallas_call(
            functools.partial(mixer, n_sp, n_tp),
            out_shape=jax.ShapeDtypeStruct((tokens, feat), BF16),
            in_specs=[vmem] * 5,
            out_specs=vmem,
            scratch_shapes=[
                pltpu.VMEM((layers, CHUNKS, n_tp, ct, feat), BF16),
                pltpu.VMEM((layers, CHUNKS, n_tp, ct, chan), BF16),
                pltpu.VMEM((tokens, n_tp * feat), BF16),
                pltpu.VMEM((layers, rows, chan + feat), BF16),
                pltpu.VMEM((layers, rows, chan), BF16),
                pltpu.VMEM((layers, tokens, chan), BF16),
                pltpu.VMEM((layers, 2, tokens, chan), BF16),
                pltpu.VMEM((3, tokens, tokens), BF16),
                pltpu.VMEM((tokens, chan), F32),
                pltpu.VMEM((tokens, feat), F32),
                pltpu.VMEM((tokens, 128), F32),
                pltpu.VMEM((layers, rows_w, chan), BF16),
                dma((layers, 2, half_tp, CHUNKS)),
                dma((layers, 2, half_tp, CHUNKS)),
                dma((layers, 2, half_z)),
                dma((layers, 2, half_z)),
                dma((layers, 2)),
                dma((2, layers)),
                dma,
                dma((layers,)),
                dma((layers,)),
                dma((layers,)),
                dma((layers,)),
                dma((2, layers)),
                dma((layers, 2)),
                dma,
            ],
            compiler_params=pltpu.CompilerParams(
                collective_id=0, has_side_effects=True, vmem_limit_bytes=48 * 1024 * 1024),
        )(tokens_in, norm_gain.reshape(layers, 1, -1), w_pool_in, w_gate, w_back)

    return jax.shard_map(
        on_device,
        mesh=mesh,
        in_specs=(
            P(("grp", "sp"), "tp"),
            P(),
            P(None, "sp", "tp"),
            P(None, "sp", "tp"),
            P(None, "tp", "sp"),
        ),
        out_specs=P(("grp", "sp"), "tp"),
        check_vma=False,
    )
```

time: 340 us -> 176 us (0.52)
  waiting for transfers between devices: 183 us -> 0 us
  Pallas kernels: 0 us -> 172 us
  blocking collectives: 62.9 us -> 0 us
  starting transfers between devices: 41.8 us -> 0 us
  local copies, waits for them, and re-layouts: 18 us -> 3.29 us
  between operations: 13.8 us -> 0.05 us
  matrix products: 12.4 us -> 0 us
  other arithmetic: 7.52 us -> 0 us
    pallas_call x0 -> x1, Pallas kernels: none -> 172 us  [on_device(): pl.pallas_call(functools.partial(mixer, n_sp, n_tp), out_shape=jax.ShapeD...]
    all_to_all x4 -> x0, waiting for transfers between devices: 95.2 us -> none  [the longest x3 70.9 us: copy_for_each(): lax.all_to_all(jnp.broadcast_to(value[None], (peers, *value.shape)), axis...]
    all_gather x1 -> x0, waiting for transfers between devices: 84.4 us -> none  [rows_first(): out, at, outs = (lax.all_gather(both, axis, axis=0, tiled=True), 0, [])]
    all_to_all x2 -> x0, blocking collectives: 62.9 us -> none  [sum_at_owner(): lax.all_to_all(parts, axis, split_axis=0, concat_axis=0, tiled=True)]
    all_to_all x4 -> x0, starting transfers between devices: 22 us -> none  [the longest x3 15.4 us: copy_for_each(): lax.all_to_all(jnp.broadcast_to(value[None], (peers, *value.shape)), axis...]
    ppermute x6 -> x0, starting transfers between devices: 19.8 us -> none  [the longest x3 11.6 us: padded_2(): after = lax.ppermute(initial, axis, down)]
    dot_general x9 -> x0, matrix products: 12.4 us -> none  [the longest x3 6.23 us: on_device(): jnp.dot(normed, gathered[1][layer_id], preferred_element_type=jnp.float32)]
    slice x7 -> x0, local copies, waits for them, and re-layouts: 9.55 us -> none  [the longest x6 9.49 us: rows_first(): section = out[:, at:at + t[0].size].reshape(-1, *t.shape[1:])]
  transfers between devices with their start and end apart: 11 -> 0, of which waited for: 8 -> 0; matrix products, arithmetic and copies ran while one was open for 2% -> 0% of each run, Pallas kernels for 0% -> 0%
where the time goes in v1:
time: 176 us
  Pallas kernels  172 us (98%)
  local copies, waits for them, and re-layouts  3.29 us (2%)
    pallas_call x1, Pallas kernels, on_device(): pl.pallas_call(functools.partial(mixer, n_sp, n_tp), out_shape=jax.ShapeD...  172 us

profile of v1, /device:TPU:65, one launch (start us, length us, event | category | flops | bytes accessed | tf_op | source)
XLA Modules:
  0.0 175.7 jit_solution(11495988684380007677)
XLA Ops:
  0.0 0.0 copy-start
  0.0 0.8 reshape.3.gain_ref
  0.8 0.0 copy-start.2
  0.8 0.9 copy.6.wback_ref
  1.8 0.0 copy-done
  1.8 0.0 copy-done.2
  1.8 0.0 copy-start.1
  1.8 0.9 copy-done.1
  2.7 172.4 %shard_map.55 = bf16[256,256]{1,0:T(8,128)(2,1)S(1)} custom-call(bf16[256,256]{1,0:T(8,128)(2,1)S(1)} %copy-done, f32[3,1,2048]{2,1,0:T(1,128)S(1)} %reshape.3.gain_ref, bf16[3,64,128]{2,1,0:T(8,128)(2,1)S(1)} %copy-done.2, bf16[3,64,256]{2,1,0:T(8,128)(2,1)S(1)} %copy-done.1, bf16[3,128,64]{2,1,0:T(8,128)(2,1)S(1)} %copy.6.wback_ref), custom_call_target="tpu_custom_call" | custom-call | tf_op jit(solution)/shard_map/pallas_call | solution.py:337
  175.1 0.7 copy.8
Async XLA Ops:
  0.0 1.8 %copy-start = (bf16[256,256]{1,0:T(8,128)(2,1)S(1)}, bf16[256,256]{1,0:T(8,128)(2,1)}, u32[]{:S(2)}) copy-start(bf16[256,256]{1,0:T(8,128)(2,1)} %tok_ref.1) | copy-start | bytes 393220
  0.8 1.0 copy-start.2
  1.8 0.9 copy-start.1

commit v2 on v1

v2 whole, which is shorter than its diff:
```python
import functools

import jax
import jax.numpy as jnp
from jax import lax
from jax.experimental import pallas as pl
from jax.experimental.pallas import tpu as pltpu
from jax.sharding import PartitionSpec as P

MESH = pl.DeviceIdType.MESH
F32 = jnp.float32
BF16 = jnp.bfloat16
GRID_W = 32
GROUPS = 4
EPS = 1e-6
CHUNKS = 2
scope = jax.named_scope

RING = {1: 0, 2: 1, 3: 2, 4: 3}
PAIRS = {1: 0, 2: 0, 3: 2, 4: 2, 5: 4, 6: 4, 7: 6, 8: 6}
FOURS = {1: 0, 2: 0, 3: 0, 4: 0, 5: 4, 6: 4, 7: 4, 8: 4}
STATE_TREE = RING
POOLED_TREE = PAIRS
POOL_W, GATE_W, BACK_W = 0, 1, 2


def weight_tree(kind, l):
    if l == 0 or kind == BACK_W:
        return FOURS
    return PAIRS


def depth(tree, d):
    return 0 if d == 0 else 1 + depth(tree, tree[d])


def stages(tree, most):
    deep = max(depth(tree, d) for d in range(1, most + 1))
    return [sorted((d for d in range(1, most + 1) if depth(tree, d) == k), reverse=True)
            for k in range(1, deep + 1)]


def children(tree, d0, most):
    return [d for d in range(most, 0, -1) if tree[d] == d0]


def mixer(n_sp, n_tp, tok_ref, gain_in, wpool_ref, wgate_ref, wback_ref, out_ref,
          xs, ps, xg, w_p, w_g, w_b, pin, halo, boxm, inv_count, gate, sumsq, gain_ref,
          x_recv, p_recv, w_recv, halo_recv, peer_recv, swap_recv,
          x_send, p_send, w_send, peer_send, halo_send, swap_send, load_sem):
    layers = gain_ref.shape[0]
    tokens, feat = tok_ref.shape
    chan = wpool_ref.shape[2]
    rows_w = wpool_ref.shape[1]
    ct = tokens // CHUNKS
    half_tp = n_tp // 2
    n_z = n_sp // 2
    half_z = n_z // 2
    q_n = n_sp // n_tp
    sp = lax.axis_index("sp")
    tp = lax.axis_index("tp")

    def tp_at(d):
        return lax.rem(tp + (d + n_tp), n_tp)

    def sp_at(d):
        return lax.rem(sp + (2 * d + n_sp), n_sp)

    peer = sp + 1 - 2 * lax.rem(sp, 2)
    before = lax.rem(sp + n_sp - 1, n_sp)
    after = lax.rem(sp + 1, n_sp)
    quad = lax.rem(sp, q_n)
    swap_to = (q_n * lax.rem(tp + half_tp, n_tp) + quad, sp // q_n)
    swap_from = (q_n * tp + quad, lax.rem(sp // q_n + half_tp, n_tp))

    def jumps(trees, most):
        return sorted({d - tree[d] for tree in trees for d in range(1, most + 1)})

    barrier = pltpu.get_barrier_semaphore()
    greet = [{"sp": before}, {"sp": after}, {"sp": swap_from[0], "tp": swap_from[1]}]
    for j in jumps((STATE_TREE, POOLED_TREE), half_tp):
        greet += [{"tp": tp_at(j)}, {"tp": tp_at(-j)}]
    for j in jumps((PAIRS, FOURS), half_z):
        greet += [{"sp": sp_at(j)}, {"sp": sp_at(-j)}]
    for who in greet:
        pl.semaphore_signal(barrier, inc=1, device_id=who, device_id_type=MESH)

    def start(src, dst, send, recv, who):
        pltpu.make_async_remote_copy(src_ref=src, dst_ref=dst, send_sem=send, recv_sem=recv,
                                     device_id=who, device_id_type=MESH).start()

    def arrived(ref, sem, name="wait"):
        with scope(name):
            pltpu.make_async_copy(ref, ref, sem).wait()

    own_rows = pl.ds(pl.multiple_of(sp * rows_w, rows_w), rows_w)
    loads = [pltpu.make_async_copy(wpool_ref, w_p.at[:, own_rows], load_sem.at[0])]
    for c in range(CHUNKS):
        loads.append(pltpu.make_async_copy(tok_ref.at[pl.ds(c * ct, ct)], xs.at[0, c, tp], load_sem.at[1 + c]))
    loads.append(pltpu.make_async_copy(wgate_ref, w_g.at[:, own_rows], load_sem.at[1 + CHUNKS]))
    loads.append(pltpu.make_async_copy(gain_in, gain_ref, load_sem.at[2 + CHUNKS]))
    for load in loads:
        load.start()

    with scope("boxes"):
        window = lax.shift_left(2, (tp * chan) // (n_tp * chan // GROUPS))
        reach_w = window // 2
        grid_rows = tokens // GRID_W
        first = sp * grid_rows
        total = grid_rows * n_sp
        ti = lax.broadcasted_iota(jnp.int32, (tokens, tokens), 0)
        tj = lax.broadcasted_iota(jnp.int32, (tokens, tokens), 1)
        ri, ci = ti // GRID_W, ti % GRID_W
        cj = tj % GRID_W
        col_in = (cj >= ci - reach_w) & (cj < ci + reach_w)
        for k in range(3):
            rj = tj // GRID_W + (k - 1) * grid_rows
            inside = col_in & (rj >= ri - reach_w) & (rj < ri + reach_w)
            boxm[k] = jnp.where(inside, 1.0, 0.0).astype(BF16)
        tr = lax.broadcasted_iota(jnp.int32, (tokens, chan), 0)
        r_at, c_at = tr // GRID_W + first, tr % GRID_W
        r_n = jnp.minimum(r_at + reach_w, total) - jnp.maximum(r_at - reach_w, 0)
        c_n = jnp.minimum(c_at + reach_w, GRID_W) - jnp.maximum(c_at - reach_w, 0)
        inv_count[...] = 1.0 / (r_n * c_n).astype(F32)

        @pl.when(sp == 0)
        def _():
            for l in range(layers):
                halo[l, 0] = jnp.zeros((tokens, chan), BF16)

        @pl.when(sp == n_sp - 1)
        def _():
            for l in range(layers):
                halo[l, 1] = jnp.zeros((tokens, chan), BF16)

    with scope("barrier"):
        pl.semaphore_wait(barrier, len(greet))

    def reach(way, c):
        if half_tp * 2 == n_tp and (c % 2 == 0) != (way == 0):
            return half_tp - 1
        return half_tp

    def x_parts(buf):
        return (STATE_TREE, x_send, x_recv) if buf is xs else (POOLED_TREE, p_send, p_recv)

    def x_forward(buf, l, c, d0, way):
        tree, send, recv = x_parts(buf)
        step = 1 if way == 0 else -1
        block = buf.at[l, c, tp_at(-step * d0)]
        for d in children(tree, d0, reach(way, c)):
            start(block, block, send.at[l], recv.at[l, way, d - 1, c], {"tp": tp_at(step * (d - d0))})

    def x_wait(buf, l, c, d, way):
        recv = x_parts(buf)[2]
        step = 1 if way == 0 else -1
        arrived(buf.at[l, c, tp_at(-step * d)], recv.at[l, way, d - 1, c], f"x{'sp'[buf is ps]}{l}_d{d}_c{c}_w{way}")

    pieces = (w_p, w_g, w_b)

    def z_reach(way):
        return half_z if way == 0 else n_z - 1 - half_z

    def z_piece(kind, l, d):
        return pieces[kind].at[l, pl.ds(pl.multiple_of(sp_at(d) * rows_w, rows_w), rows_w)]

    def z_forward(kind, l, d0, way):
        step = 1 if way == 0 else -1
        piece = z_piece(kind, l, -step * d0)
        for d in children(weight_tree(kind, l), d0, z_reach(way)):
            start(piece, piece, w_send.at[kind, l], w_recv.at[kind, l, way, d - 1], {"sp": sp_at(step * (d - d0))})

    def z_peer(kind, l, d):
        piece = z_piece(kind, l, d)
        start(piece, piece, peer_send.at[kind, l], peer_recv.at[kind, l], {"sp": peer})

    def z_begin(kind, l):
        for way in (0, 1):
            z_forward(kind, l, 0, way)
        z_peer(kind, l, 0)

    def z_stage(kind, l, k):
        for d in stages(weight_tree(kind, l), half_z)[k - 1]:
            for way in (0, 1):
                step = 1 if way == 0 else -1
                if d <= z_reach(way):
                    arrived(z_piece(kind, l, -step * d), w_recv.at[kind, l, way, d - 1], f"z{'pgb'[kind]}{l}_d{d}_w{way}")
                    z_forward(kind, l, d, way)
                    z_peer(kind, l, -step * d)

    def z_end(kind, l):
        arrived(pieces[kind].at[l, pl.ds(0, n_z * rows_w)], peer_recv.at[kind, l], f"peer{'pgb'[kind]}{l}")

    def back_begin():
        arrived(w_b.at[:, own_rows], swap_recv, "swap")
        z_begin(BACK_W, 0)

    plan = {}

    def at(l, slot, *action):
        plan.setdefault((l, slot), []).append(action)

    at(0, "S2", z_stage, POOL_W, 0, 1)
    at(0, "S4", z_stage, POOL_W, 0, 2)
    at(0, "S4", z_end, POOL_W, 0)
    at(0, "S4", back_begin)
    at(0, "H", z_stage, GATE_W, 0, 1)
    at(0, "P1", z_stage, BACK_W, 0, 1)
    at(0, "P1", z_stage, GATE_W, 0, 2)
    at(0, "P1", z_end, GATE_W, 0)
    at(0, "P2", z_stage, BACK_W, 0, 2)
    at(0, "P2", z_end, BACK_W, 0)
    for l in range(1, layers):
        for kind in (POOL_W, GATE_W):
            at(l - 1, "H", z_begin, kind, l)
            at(l - 1, "P2", z_stage, kind, l, 1)
            at(l, "S1", z_stage, kind, l, 2)
            at(l, "S3", z_stage, kind, l, 3)
            at(l, "S4", z_stage, kind, l, 4)
            at(l, "S4", z_end, kind, l)
        at(l, "S1", z_begin, BACK_W, l)
        at(l, "S4", z_stage, BACK_W, l, 1)
        at(l, "P2", z_stage, BACK_W, l, 2)
        at(l, "P2", z_end, BACK_W, l)

    def slot(l, name):
        for action in plan.get((l, name), ()):
            action[0](*action[1:])

    def prep(l, c, j):
        block = xs[l, c, j].astype(F32)
        lanes = pl.ds(pl.multiple_of(j * feat, feat), feat)
        squares = block * block
        part = squares[:, 0:128]
        for k in range(1, feat // 128):
            part = part + squares[:, k * 128:(k + 1) * 128]
        sumsq[c * ct:(c + 1) * ct, :] += part
        xg[c * ct:(c + 1) * ct, lanes] = (block * gain_ref[l:l + 1, lanes]).astype(BF16)

    loads[0].wait()
    z_begin(POOL_W, 0)
    for c in range(CHUNKS):
        loads[1 + c].wait()
        for way in (0, 1):
            x_forward(xs, 0, c, 0, way)
    loads[1 + CHUNKS].wait()
    start(wback_ref, w_b.at[:, pl.ds(pl.multiple_of(swap_to[0] * rows_w, rows_w), rows_w)], swap_send, swap_recv,
          {"sp": swap_to[0], "tp": swap_to[1]})
    z_begin(GATE_W, 0)
    loads[2 + CHUNKS].wait()

    def x_gather(buf, l, name, each, last):
        deep = stages(x_parts(buf)[0], half_tp)
        for k, ds in enumerate(deep, 1):
            if k == len(deep) and last is not None:
                slot(l, f"{name}{k}")
            for c in range(CHUNKS):
                got = []
                for d in ds:
                    for way in (0, 1):
                        if d <= reach(way, c):
                            x_wait(buf, l, c, d, way)
                            x_forward(buf, l, c, d, way)
                            got.append(-d if way == 0 else d)
                if each is not None:
                    for d in got:
                        each(c, tp_at(d))
                if k == len(deep) and last is not None:
                    last(c)
            if k < len(deep) or last is None:
                slot(l, f"{name}{k}")

    for l in range(layers):
        sumsq[...] = jnp.zeros_like(sumsq)
        for c in range(CHUNKS):
            prep(l, c, tp)
        x_gather(xs, l, "S", functools.partial(prep, l), None)

        scale = lax.rsqrt(jnp.sum(sumsq[...], axis=1, keepdims=True) * (1.0 / (n_tp * feat)) + EPS)
        pool = jnp.dot(xg[...], w_p[l], preferred_element_type=F32)
        pin[l] = (pool * scale).astype(BF16)

        @pl.when(sp > 0)
        def _():
            start(pin.at[l], halo.at[l, 1], halo_send.at[l, 1], halo_recv.at[l, 1], {"sp": before})

        @pl.when(sp < n_sp - 1)
        def _():
            start(pin.at[l], halo.at[l, 0], halo_send.at[l, 0], halo_recv.at[l, 0], {"sp": after})

        def make_gate():
            rows_scale = lax.rsqrt(jnp.sum(sumsq[...], axis=1, keepdims=True) * (1.0 / (n_tp * feat)) + EPS)
            gate_acc = jnp.dot(xg[...], w_g[l], preferred_element_type=F32)
            gate[...] = jax.nn.sigmoid(gate_acc * rows_scale)

        slot(l, "H")
        if l > 0:
            make_gate()
        own_pool = pin[l]
        box = jnp.dot(boxm[1], own_pool, preferred_element_type=F32)

        @pl.when(sp > 0)
        def _():
            arrived(halo.at[l, 0], halo_recv.at[l, 0], f"halo{l}_0")

        @pl.when(sp < n_sp - 1)
        def _():
            arrived(halo.at[l, 1], halo_recv.at[l, 1], f"halo{l}_1")

        box = box + jnp.dot(boxm[0], halo[l, 0], preferred_element_type=F32)
        box = box + jnp.dot(boxm[2], halo[l, 1], preferred_element_type=F32)
        pooled = (box * inv_count[...] - own_pool.astype(F32)).astype(BF16)
        for c in range(CHUNKS):
            ps[l, c, tp] = pooled[c * ct:(c + 1) * ct]
            for way in (0, 1):
                x_forward(ps, l, c, 0, way)

        def finish(c):
            if l == 0 and c == 0:
                make_gate()
            branch = None
            for p in range(n_tp):
                term = lax.dot_general(ps[l, c, (p + half_tp) % n_tp], w_b[l, p * feat:(p + 1) * feat],
                                       (((1,), (1,)), ((), ())), preferred_element_type=F32)
                branch = term if branch is None else branch + term
            rows = slice(c * ct, (c + 1) * ct)
            new = (xs[l, c, tp].astype(F32) + gate[rows] * branch).astype(BF16)
            if l + 1 < layers:
                xs[l + 1, c, tp] = new
                for way in (0, 1):
                    x_forward(xs, l + 1, c, 0, way)
            else:
                out_ref[rows, :] = new

        x_gather(ps, l, "P", None, finish)

    arrived(wback_ref, swap_send)

    def drained(ref, rows, sem):
        while rows:
            now = min(rows, ref.shape[0])
            arrived(ref.at[pl.ds(0, now)], sem)
            rows -= now

    sent = {buf_i: sum(reach(way, c) for way in (0, 1) for c in range(CHUNKS)) for buf_i in (0, 1)}
    for l in range(layers):
        for buf, send in ((xs, x_send), (ps, p_send)):
            left = sent[0]
            c = 0
            while left:
                now = min(left, n_tp)
                arrived(buf.at[l, c % CHUNKS, pl.ds(0, now)], send.at[l])
                left -= now
                c += 1
        for kind in range(3):
            drained(pieces[kind].at[l], (z_reach(0) + z_reach(1)) * rows_w, w_send.at[kind, l])
            drained(pieces[kind].at[l], n_z * rows_w, peer_send.at[kind, l])

        @pl.when(sp > 0)
        def _():
            arrived(pin.at[l], halo_send.at[l, 1])

        @pl.when(sp < n_sp - 1)
        def _():
            arrived(pin.at[l], halo_send.at[l, 0])


def solution(mesh):
    n_sp, n_tp = mesh.shape["sp"], mesh.shape["tp"]

    def on_device(tokens_in, norm_gain, w_pool_in, w_gate, w_back):
        layers = norm_gain.shape[0]
        tokens, feat = tokens_in.shape
        rows_w, chan = w_pool_in.shape[1:]
        rows = n_sp * rows_w
        ct = tokens // CHUNKS
        half_tp = n_tp // 2
        half_z = n_sp // 4
        dma = pltpu.SemaphoreType.DMA
        return pl.pallas_call(
            functools.partial(mixer, n_sp, n_tp),
            out_shape=jax.ShapeDtypeStruct((tokens, feat), BF16),
            in_specs=[pl.BlockSpec(memory_space=pltpu.HBM)] * 5,
            out_specs=pl.BlockSpec(memory_space=pltpu.VMEM),
            scratch_shapes=[
                pltpu.VMEM((layers, CHUNKS, n_tp, ct, feat), BF16),
                pltpu.VMEM((layers, CHUNKS, n_tp, ct, chan), BF16),
                pltpu.VMEM((tokens, n_tp * feat), BF16),
                pltpu.VMEM((layers, rows, chan), BF16),
                pltpu.VMEM((layers, rows, feat), BF16),
                pltpu.VMEM((layers, rows, chan), BF16),
                pltpu.VMEM((layers, tokens, chan), BF16),
                pltpu.VMEM((layers, 2, tokens, chan), BF16),
                pltpu.VMEM((3, tokens, tokens), BF16),
                pltpu.VMEM((tokens, chan), F32),
                pltpu.VMEM((tokens, feat), F32),
                pltpu.VMEM((tokens, 128), F32),
                pltpu.VMEM(norm_gain.shape, F32),
                dma((layers, 2, half_tp, CHUNKS)),
                dma((layers, 2, half_tp, CHUNKS)),
                dma((3, layers, 2, half_z)),
                dma((layers, 2)),
                dma((3, layers)),
                dma,
                dma((layers,)),
                dma((layers,)),
                dma((3, layers)),
                dma((3, layers)),
                dma((layers, 2)),
                dma,
                dma((3 + CHUNKS,)),
            ],
            compiler_params=pltpu.CompilerParams(
                collective_id=0, has_side_effects=True, vmem_limit_bytes=67043328),
        )(tokens_in, norm_gain, w_pool_in, w_gate, jnp.swapaxes(w_back, 1, 2))

    return jax.shard_map(
        on_device,
        mesh=mesh,
        in_specs=(
            P(("grp", "sp"), "tp"),
            P(),
            P(None, "sp", "tp"),
            P(None, "sp", "tp"),
            P(None, "tp", "sp"),
        ),
        out_specs=P(("grp", "sp"), "tp"),
        check_vma=False,
    )
```

time: 176 us -> 167 us (0.949)
  Pallas kernels: 172 us -> 165 us
    pallas_call x1, Pallas kernels: 172 us -> 165 us  [on_device(): pl.pallas_call(functools.partial(mixer, n_sp, n_tp), out_shape=jax.ShapeD...]
where the time goes in v2:
time: 167 us
  Pallas kernels  165 us (99%)
    pallas_call x1, Pallas kernels, on_device(): pl.pallas_call(functools.partial(mixer, n_sp, n_tp), out_shape=jax.ShapeD...  165 us

profile of v2, /device:TPU:65, one launch (start us, length us, event | category | flops | bytes accessed | tf_op | source)
XLA Modules:
  0.0 166.7 jit_solution(7697886537728827243)
XLA Ops:
  0.0 165.1 %shard_map.55 = bf16[256,256]{1,0:T(8,128)(2,1)} custom-call(bf16[256,256]{1,0:T(8,128)(2,1)} %tok_ref.1, f32[3,2048]{1,0:T(4,128)} %gain_in.1, bf16[3,64,128]{2,1,0:T(8,128)(2,1)} %wpool_ref.1, bf16[3,64,256]{2,1,0:T(8,128)(2,1)} %wgate_ref.1, bf16[3,64,128]{2,1,0:T(8,128)(2,1)} %bitcast.1), custom_call_target="tpu_custom_call" | custom-call | tf_op jit(solution)/shard_map/pallas_call | solution.py:380
  165.1 1.6 copy.7

commit v3 on v2

--- a/solution.py
+++ b/solution.py
@@ -25,7 +25,7 @@
 
 
 def weight_tree(kind, l):
-    if l == 0 or kind == BACK_W:
+    if l == 0:
         return FOURS
     return PAIRS
 
@@ -201,27 +201,21 @@
         plan.setdefault((l, slot), []).append(action)
 
     at(0, "S2", z_stage, POOL_W, 0, 1)
+    at(0, "S3", back_begin)
     at(0, "S4", z_stage, POOL_W, 0, 2)
     at(0, "S4", z_end, POOL_W, 0)
-    at(0, "S4", back_begin)
-    at(0, "H", z_stage, GATE_W, 0, 1)
-    at(0, "P1", z_stage, BACK_W, 0, 1)
-    at(0, "P1", z_stage, GATE_W, 0, 2)
-    at(0, "P1", z_end, GATE_W, 0)
+    at(0, "I", z_stage, GATE_W, 0, 1)
+    at(0, "I", z_stage, BACK_W, 0, 1)
+    at(0, "P2", z_stage, GATE_W, 0, 2)
     at(0, "P2", z_stage, BACK_W, 0, 2)
+    at(0, "P2", z_end, GATE_W, 0)
     at(0, "P2", z_end, BACK_W, 0)
     for l in range(1, layers):
-        for kind in (POOL_W, GATE_W):
-            at(l - 1, "H", z_begin, kind, l)
-            at(l - 1, "P2", z_stage, kind, l, 1)
-            at(l, "S1", z_stage, kind, l, 2)
-            at(l, "S3", z_stage, kind, l, 3)
-            at(l, "S4", z_stage, kind, l, 4)
-            at(l, "S4", z_end, kind, l)
-        at(l, "S1", z_begin, BACK_W, l)
-        at(l, "S4", z_stage, BACK_W, l, 1)
-        at(l, "P2", z_stage, BACK_W, l, 2)
-        at(l, "P2", z_end, BACK_W, l)
+        kinds = (POOL_W, GATE_W, BACK_W)
+        for where, action, *more in (((l - 1, "I"), z_begin), ((l - 1, "P2"), z_stage, 1), ((l, "S1"), z_stage, 2),
+                                     ((l, "S2"), z_stage, 3), ((l, "S3"), z_stage, 4), ((l, "S4"), z_end)):
+            for kind in kinds:
+                at(*where, action, kind, l, *more)
 
     def slot(l, name):
         for action in plan.get((l, name), ()):
@@ -267,8 +261,11 @@
                         each(c, tp_at(d))
                 if k == len(deep) and last is not None:
                     last(c)
-            if k < len(deep) or last is None:
+            if k < len(deep):
                 slot(l, f"{name}{k}")
+            elif last is None:
+                for rest in range(k, 5):
+                    slot(l, f"{name}{rest}")
 
     for l in range(layers):
         sumsq[...] = jnp.zeros_like(sumsq)
@@ -293,7 +290,6 @@
             gate_acc = jnp.dot(xg[...], w_g[l], preferred_element_type=F32)
             gate[...] = jax.nn.sigmoid(gate_acc * rows_scale)
 
-        slot(l, "H")
         if l > 0:
             make_gate()
         own_pool = pin[l]
@@ -314,6 +310,7 @@
             ps[l, c, tp] = pooled[c * ct:(c + 1) * ct]
             for way in (0, 1):
                 x_forward(ps, l, c, 0, way)
+        slot(l, "I")
 
         def finish(c):
             if l == 0 and c == 0:

time: 167 us -> 159 us (0.952)
  Pallas kernels: 165 us -> 157 us
    pallas_call x1, Pallas kernels: 165 us -> 157 us  [on_device(): pl.pallas_call(functools.partial(mixer, n_sp, n_tp), out_shape=jax.ShapeD...]
where the time goes in v3:
time: 159 us
  Pallas kernels  157 us (99%)
    pallas_call x1, Pallas kernels, on_device(): pl.pallas_call(functools.partial(mixer, n_sp, n_tp), out_shape=jax.ShapeD...  157 us

profile of v3, /device:TPU:65, one launch (start us, length us, event | category | flops | bytes accessed | tf_op | source)
XLA Modules:
  0.0 158.5 jit_solution(12952864613172575694)
XLA Ops:
  0.0 156.9 %shard_map.55 = bf16[256,256]{1,0:T(8,128)(2,1)} custom-call(bf16[256,256]{1,0:T(8,128)(2,1)} %tok_ref.1, f32[3,2048]{1,0:T(4,128)} %gain_in.1, bf16[3,64,128]{2,1,0:T(8,128)(2,1)} %wpool_ref.1, bf16[3,64,256]{2,1,0:T(8,128)(2,1)} %wgate_ref.1, bf16[3,64,128]{2,1,0:T(8,128)(2,1)} %bitcast.1), custom_call_target="tpu_custom_call" | custom-call | tf_op jit(solution)/shard_map/pallas_call | solution.py:377
  157.0 1.6 copy.7

commit v4 on v3

--- a/solution.py
+++ b/solution.py
@@ -25,7 +25,7 @@
 
 
 def weight_tree(kind, l):
-    if l == 0:
+    if l == 0 and kind == POOL_W:
         return FOURS
     return PAIRS
 
@@ -45,7 +45,7 @@
 
 
 def mixer(n_sp, n_tp, tok_ref, gain_in, wpool_ref, wgate_ref, wback_ref, out_ref,
-          xs, ps, xg, w_p, w_g, w_b, pin, halo, boxm, inv_count, gate, sumsq, gain_ref,
+          xs, ps, xg, w_p, w_g, w_b, pin, halo, boxm, inv_count, gate, sumsq, gain_ref, pool_acc,
           x_recv, p_recv, w_recv, halo_recv, peer_recv, swap_recv,
           x_send, p_send, w_send, peer_send, halo_send, swap_send, load_sem):
     layers = gain_ref.shape[0]
@@ -192,8 +192,11 @@
         arrived(pieces[kind].at[l, pl.ds(0, n_z * rows_w)], peer_recv.at[kind, l], f"peer{'pgb'[kind]}{l}")
 
     def back_begin():
-        arrived(w_b.at[:, own_rows], swap_recv, "swap")
+        arrived(w_b.at[0, own_rows], swap_recv.at[0], "swap")
         z_begin(BACK_W, 0)
+
+    def swap_rest():
+        arrived(w_b.at[pl.ds(1, layers - 1), own_rows], swap_recv.at[1], "swap")
 
     plan = {}
 
@@ -201,21 +204,36 @@
         plan.setdefault((l, slot), []).append(action)
 
     at(0, "S2", z_stage, POOL_W, 0, 1)
-    at(0, "S3", back_begin)
+    at(0, "S2", back_begin)
+    at(0, "S2", z_stage, GATE_W, 0, 1)
+    at(0, "S3", z_stage, GATE_W, 0, 2)
+    at(0, "S3", z_stage, BACK_W, 0, 1)
     at(0, "S4", z_stage, POOL_W, 0, 2)
+    at(0, "S4", z_stage, BACK_W, 0, 2)
     at(0, "S4", z_end, POOL_W, 0)
-    at(0, "I", z_stage, GATE_W, 0, 1)
-    at(0, "I", z_stage, BACK_W, 0, 1)
-    at(0, "P2", z_stage, GATE_W, 0, 2)
-    at(0, "P2", z_stage, BACK_W, 0, 2)
+    at(0, "I", z_stage, GATE_W, 0, 3)
+    at(0, "I", z_stage, BACK_W, 0, 3)
+    at(0, "P1", z_stage, GATE_W, 0, 4)
+    at(0, "P1", z_stage, BACK_W, 0, 4)
     at(0, "P2", z_end, GATE_W, 0)
     at(0, "P2", z_end, BACK_W, 0)
+    at(0, "I", swap_rest)
     for l in range(1, layers):
-        kinds = (POOL_W, GATE_W, BACK_W)
-        for where, action, *more in (((l - 1, "I"), z_begin), ((l - 1, "P2"), z_stage, 1), ((l, "S1"), z_stage, 2),
-                                     ((l, "S2"), z_stage, 3), ((l, "S3"), z_stage, 4), ((l, "S4"), z_end)):
-            for kind in kinds:
-                at(*where, action, kind, l, *more)
+        for kind in (POOL_W, GATE_W, BACK_W):
+            at(l - 1, "I", z_begin, kind, l)
+        for kind in (POOL_W, GATE_W, BACK_W):
+            at(l - 1, "P1", z_stage, kind, l, 1)
+        for kind in (POOL_W, GATE_W, BACK_W):
+            at(l, "S1", z_stage, kind, l, 2)
+        at(l, "S2", z_stage, POOL_W, l, 3)
+        at(l, "S3", z_stage, POOL_W, l, 4)
+        at(l, "S3", z_stage, GATE_W, l, 3)
+        at(l, "S3", z_stage, BACK_W, l, 3)
+        at(l, "S3", z_end, POOL_W, l)
+        at(l, "I", z_stage, GATE_W, l, 4)
+        at(l, "I", z_stage, BACK_W, l, 4)
+        at(l, "P2", z_end, GATE_W, l)
+        at(l, "P2", z_end, BACK_W, l)
 
     def slot(l, name):
         for action in plan.get((l, name), ()):
@@ -231,23 +249,37 @@
         sumsq[c * ct:(c + 1) * ct, :] += part
         xg[c * ct:(c + 1) * ct, lanes] = (block * gain_ref[l:l + 1, lanes]).astype(BF16)
 
-    loads[0].wait()
-    z_begin(POOL_W, 0)
+    swap_rows = pl.ds(pl.multiple_of(swap_to[0] * rows_w, rows_w), rows_w)
+    swap_who = {"sp": swap_to[0], "tp": swap_to[1]}
+    start(wback_ref.at[0], w_b.at[0, swap_rows], swap_send.at[0], swap_recv.at[0], swap_who)
     for c in range(CHUNKS):
         loads[1 + c].wait()
         for way in (0, 1):
             x_forward(xs, 0, c, 0, way)
+    loads[0].wait()
+    z_begin(POOL_W, 0)
     loads[1 + CHUNKS].wait()
-    start(wback_ref, w_b.at[:, pl.ds(pl.multiple_of(swap_to[0] * rows_w, rows_w), rows_w)], swap_send, swap_recv,
-          {"sp": swap_to[0], "tp": swap_to[1]})
     z_begin(GATE_W, 0)
+    rest = pl.ds(1, layers - 1)
+    start(wback_ref.at[rest], w_b.at[rest, swap_rows], swap_send.at[1], swap_recv.at[1], swap_who)
     loads[2 + CHUNKS].wait()
+
+    def pool_term(l, d):
+        at_d = pl.ds(pl.multiple_of(tp_at(d) * feat, feat), feat)
+        return jnp.dot(xg[:, at_d], w_p[l, at_d], preferred_element_type=F32)
+
+    def ahead(l):
+        if l > 0:
+            total_here = pool_term(l, 0)
+            for d in range(1, half_tp):
+                total_here = total_here + pool_term(l, d) + pool_term(l, -d)
+            pool_acc[...] = total_here
 
     def x_gather(buf, l, name, each, last):
         deep = stages(x_parts(buf)[0], half_tp)
         for k, ds in enumerate(deep, 1):
-            if k == len(deep) and last is not None:
-                slot(l, f"{name}{k}")
+            if k == len(deep) and last is None:
+                ahead(l)
             for c in range(CHUNKS):
                 got = []
                 for d in ds:
@@ -260,6 +292,8 @@
                     for d in got:
                         each(c, tp_at(d))
                 if k == len(deep) and last is not None:
+                    if c == 0:
+                        slot(l, f"{name}{k}")
                     last(c)
             if k < len(deep):
                 slot(l, f"{name}{k}")
@@ -274,7 +308,10 @@
         x_gather(xs, l, "S", functools.partial(prep, l), None)
 
         scale = lax.rsqrt(jnp.sum(sumsq[...], axis=1, keepdims=True) * (1.0 / (n_tp * feat)) + EPS)
-        pool = jnp.dot(xg[...], w_p[l], preferred_element_type=F32)
+        if l == 0:
+            pool = jnp.dot(xg[...], w_p[l], preferred_element_type=F32)
+        else:
+            pool = pool_acc[...] + pool_term(l, half_tp)
         pin[l] = (pool * scale).astype(BF16)
 
         @pl.when(sp > 0)
@@ -290,8 +327,6 @@
             gate_acc = jnp.dot(xg[...], w_g[l], preferred_element_type=F32)
             gate[...] = jax.nn.sigmoid(gate_acc * rows_scale)
 
-        if l > 0:
-            make_gate()
         own_pool = pin[l]
         box = jnp.dot(boxm[1], own_pool, preferred_element_type=F32)
 
@@ -313,7 +348,7 @@
         slot(l, "I")
 
         def finish(c):
-            if l == 0 and c == 0:
+            if c == 0:
                 make_gate()
             branch = None
             for p in range(n_tp):
@@ -331,7 +366,8 @@
 
         x_gather(ps, l, "P", None, finish)
 
-    arrived(wback_ref, swap_send)
+    arrived(wback_ref.at[0], swap_send.at[0])
+    arrived(wback_ref.at[rest], swap_send.at[1])
 
     def drained(ref, rows, sem):
         while rows:
@@ -376,7 +412,7 @@
         dma = pltpu.SemaphoreType.DMA
         return pl.pallas_call(
             functools.partial(mixer, n_sp, n_tp),
-            out_shape=jax.ShapeDtypeStruct((tokens, feat), BF16),
+            out_shape=pltpu.VMEM((tokens, feat), BF16),
             in_specs=[pl.BlockSpec(memory_space=pltpu.HBM)] * 5,
             out_specs=pl.BlockSpec(memory_space=pltpu.VMEM),
             scratch_shapes=[
@@ -393,22 +429,23 @@
                 pltpu.VMEM((tokens, feat), F32),
                 pltpu.VMEM((tokens, 128), F32),
                 pltpu.VMEM(norm_gain.shape, F32),
+                pltpu.VMEM((tokens, chan), F32),
                 dma((layers, 2, half_tp, CHUNKS)),
                 dma((layers, 2, half_tp, CHUNKS)),
                 dma((3, layers, 2, half_z)),
                 dma((layers, 2)),
                 dma((3, layers)),
-                dma,
+                dma((2,)),
                 dma((layers,)),
                 dma((layers,)),
                 dma((3, layers)),
                 dma((3, layers)),
                 dma((layers, 2)),
-                dma,
+                dma((2,)),
                 dma((3 + CHUNKS,)),
             ],
             compiler_params=pltpu.CompilerParams(
-                collective_id=0, has_side_effects=True, vmem_limit_bytes=67043328),
+                collective_id=0, has_side_effects=True, vmem_limit_bytes=66700000),
         )(tokens_in, norm_gain, w_pool_in, w_gate, jnp.swapaxes(w_back, 1, 2))
 
     return jax.shard_map(

time: 159 us -> 147 us (0.925)
  Pallas kernels: 157 us -> 146 us
    pallas_call x1, Pallas kernels: 157 us -> 146 us  [on_device(): pl.pallas_call(functools.partial(mixer, n_sp, n_tp), out_shape=pltpu.VMEM...]
where the time goes in v4:
time: 147 us
  Pallas kernels  146 us (99%)
    pallas_call x1, Pallas kernels, on_device(): pl.pallas_call(functools.partial(mixer, n_sp, n_tp), out_shape=pltpu.VMEM...  146 us

profile of v4, /device:TPU:65, one launch (start us, length us, event | category | flops | bytes accessed | tf_op | source)
XLA Modules:
  0.0 146.9 jit_solution(9682991393988915834)
XLA Ops:
  0.0 146.3 %shard_map.55 = bf16[256,256]{1,0:T(8,128)(2,1)S(1)} custom-call(bf16[256,256]{1,0:T(8,128)(2,1)} %tok_ref.1, f32[3,2048]{1,0:T(4,128)} %gain_in.1, bf16[3,64,128]{2,1,0:T(8,128)(2,1)} %wpool_ref.1, bf16[3,64,256]{2,1,0:T(8,128)(2,1)} %wgate_ref.1, bf16[3,64,128]{2,1,0:T(8,128)(2,1)} %bitcast.1), custom_call_target="tpu_custom_call" | custom-call | tf_op jit(solution)/shard_map/pallas_call | solution.py:413
  146.3 0.7 copy.7

commit v5 on v4

--- a/solution.py
+++ b/solution.py
@@ -13,21 +13,22 @@
 GRID_W = 32
 GROUPS = 4
 EPS = 1e-6
-CHUNKS = 2
+CHUNKS = 4
 scope = jax.named_scope
 
 RING = {1: 0, 2: 1, 3: 2, 4: 3}
 PAIRS = {1: 0, 2: 0, 3: 2, 4: 2, 5: 4, 6: 4, 7: 6, 8: 6}
 FOURS = {1: 0, 2: 0, 3: 0, 4: 0, 5: 4, 6: 4, 7: 4, 8: 4}
+MIXED = {1: 0, 2: 0, 3: 0, 4: 0, 5: 4, 6: 4, 7: 6, 8: 6}
 STATE_TREE = RING
 POOLED_TREE = PAIRS
 POOL_W, GATE_W, BACK_W = 0, 1, 2
 
 
 def weight_tree(kind, l):
-    if l == 0 and kind == POOL_W:
+    if kind == POOL_W:
         return FOURS
-    return PAIRS
+    return MIXED if kind == BACK_W and l == 0 else PAIRS
 
 
 def depth(tree, d):
@@ -46,8 +47,7 @@
 
 def mixer(n_sp, n_tp, tok_ref, gain_in, wpool_ref, wgate_ref, wback_ref, out_ref,
           xs, ps, xg, w_p, w_g, w_b, pin, halo, boxm, inv_count, gate, sumsq, gain_ref, pool_acc,
-          x_recv, p_recv, w_recv, halo_recv, peer_recv, swap_recv,
-          x_send, p_send, w_send, peer_send, halo_send, swap_send, load_sem):
+          x_recv, p_recv, w_recv, halo_recv, peer_recv, swap_recv, sent, load_sem):
     layers = gain_ref.shape[0]
     tokens, feat = tok_ref.shape
     chan = wpool_ref.shape[2]
@@ -85,8 +85,8 @@
     for who in greet:
         pl.semaphore_signal(barrier, inc=1, device_id=who, device_id_type=MESH)
 
-    def start(src, dst, send, recv, who):
-        pltpu.make_async_remote_copy(src_ref=src, dst_ref=dst, send_sem=send, recv_sem=recv,
+    def start(src, dst, recv, who):
+        pltpu.make_async_remote_copy(src_ref=src, dst_ref=dst, send_sem=sent, recv_sem=recv,
                                      device_id=who, device_id_type=MESH).start()
 
     def arrived(ref, sem, name="wait"):
@@ -142,19 +142,19 @@
         return half_tp
 
     def x_parts(buf):
-        return (STATE_TREE, x_send, x_recv) if buf is xs else (POOLED_TREE, p_send, p_recv)
+        return (STATE_TREE, x_recv) if buf is xs else (POOLED_TREE, p_recv)
 
     def x_forward(buf, l, c, d0, way):
-        tree, send, recv = x_parts(buf)
+        tree, recv = x_parts(buf)
         step = 1 if way == 0 else -1
         block = buf.at[l, c, tp_at(-step * d0)]
         for d in children(tree, d0, reach(way, c)):
-            start(block, block, send.at[l], recv.at[l, way, d - 1, c], {"tp": tp_at(step * (d - d0))})
+            start(block, block, recv.at[way, d - 1, c], {"tp": tp_at(step * (d - d0))})
 
     def x_wait(buf, l, c, d, way):
-        recv = x_parts(buf)[2]
+        recv = x_parts(buf)[1]
         step = 1 if way == 0 else -1
-        arrived(buf.at[l, c, tp_at(-step * d)], recv.at[l, way, d - 1, c], f"x{'sp'[buf is ps]}{l}_d{d}_c{c}_w{way}")
+        arrived(buf.at[l, c, tp_at(-step * d)], recv.at[way, d - 1, c], f"x{'sp'[buf is ps]}{l}_d{d}_c{c}_w{way}")
 
     pieces = (w_p, w_g, w_b)
 
@@ -163,30 +163,41 @@
 
     def z_piece(kind, l, d):
         return pieces[kind].at[l, pl.ds(pl.multiple_of(sp_at(d) * rows_w, rows_w), rows_w)]
+
+    def z_group(kind, l, d):
+        tree = weight_tree(kind, l)
+        if tree is FOURS and depth(tree, d) == 1 and not children(tree, d, half_z):
+            return 2
+        return depth(tree, d) - 1
 
     def z_forward(kind, l, d0, way):
         step = 1 if way == 0 else -1
         piece = z_piece(kind, l, -step * d0)
         for d in children(weight_tree(kind, l), d0, z_reach(way)):
-            start(piece, piece, w_send.at[kind, l], w_recv.at[kind, l, way, d - 1], {"sp": sp_at(step * (d - d0))})
+            start(piece, piece, w_recv.at[kind, l, z_group(kind, l, d)], {"sp": sp_at(step * (d - d0))})
 
     def z_peer(kind, l, d):
         piece = z_piece(kind, l, d)
-        start(piece, piece, peer_send.at[kind, l], peer_recv.at[kind, l], {"sp": peer})
+        start(piece, piece, peer_recv.at[kind, l], {"sp": peer})
 
     def z_begin(kind, l):
         for way in (0, 1):
             z_forward(kind, l, 0, way)
         z_peer(kind, l, 0)
 
-    def z_stage(kind, l, k):
-        for d in stages(weight_tree(kind, l), half_z)[k - 1]:
-            for way in (0, 1):
-                step = 1 if way == 0 else -1
-                if d <= z_reach(way):
-                    arrived(z_piece(kind, l, -step * d), w_recv.at[kind, l, way, d - 1], f"z{'pgb'[kind]}{l}_d{d}_w{way}")
-                    z_forward(kind, l, d, way)
-                    z_peer(kind, l, -step * d)
+    def z_stage(kind, l, k, forwarded=None):
+        tree = weight_tree(kind, l)
+        groups = {}
+        for d in stages(tree, half_z)[k - 1]:
+            if forwarded is None or forwarded == bool(children(tree, d, half_z)):
+                groups.setdefault(z_group(kind, l, d), []).extend((d, way) for way in (0, 1) if d <= z_reach(way))
+        for group, ones in groups.items():
+            arrived(pieces[kind].at[l, pl.ds(0, len(ones) * rows_w)], w_recv.at[kind, l, group],
+                    f"z{'pgb'[kind]}{l}_{k}_{group}")
+            for d, way in ones:
+                z_forward(kind, l, d, way)
+            for d, way in ones:
+                z_peer(kind, l, -d if way == 0 else d)
 
     def z_end(kind, l):
         arrived(pieces[kind].at[l, pl.ds(0, n_z * rows_w)], peer_recv.at[kind, l], f"peer{'pgb'[kind]}{l}")
@@ -198,41 +209,47 @@
     def swap_rest():
         arrived(w_b.at[pl.ds(1, layers - 1), own_rows], swap_recv.at[1], "swap")
 
+    def norm_scale():
+        return lax.rsqrt(jnp.sum(sumsq[...], axis=1, keepdims=True) * (1.0 / (n_tp * feat)) + EPS)
+
+    def make_gate(l):
+        gate_acc = jnp.dot(xg[...], w_g[l], preferred_element_type=F32)
+        gate[...] = jax.nn.sigmoid(gate_acc * norm_scale())
+
     plan = {}
 
     def at(l, slot, *action):
         plan.setdefault((l, slot), []).append(action)
 
-    at(0, "S2", z_stage, POOL_W, 0, 1)
+    at(0, "S1", z_stage, POOL_W, 0, 1, True)
+    at(0, "S2", z_stage, GATE_W, 0, 1)
     at(0, "S2", back_begin)
-    at(0, "S2", z_stage, GATE_W, 0, 1)
-    at(0, "S3", z_stage, GATE_W, 0, 2)
-    at(0, "S3", z_stage, BACK_W, 0, 1)
+    at(0, "S3", z_stage, POOL_W, 0, 1, False)
     at(0, "S4", z_stage, POOL_W, 0, 2)
-    at(0, "S4", z_stage, BACK_W, 0, 2)
     at(0, "S4", z_end, POOL_W, 0)
+    at(0, "H", z_stage, GATE_W, 0, 2)
+    at(0, "H", z_stage, BACK_W, 0, 1)
     at(0, "I", z_stage, GATE_W, 0, 3)
-    at(0, "I", z_stage, BACK_W, 0, 3)
+    at(0, "I", z_stage, BACK_W, 0, 2)
+    at(0, "I", swap_rest)
     at(0, "P1", z_stage, GATE_W, 0, 4)
-    at(0, "P1", z_stage, BACK_W, 0, 4)
-    at(0, "P2", z_end, GATE_W, 0)
-    at(0, "P2", z_end, BACK_W, 0)
-    at(0, "I", swap_rest)
-    for l in range(1, layers):
-        for kind in (POOL_W, GATE_W, BACK_W):
-            at(l - 1, "I", z_begin, kind, l)
-        for kind in (POOL_W, GATE_W, BACK_W):
-            at(l - 1, "P1", z_stage, kind, l, 1)
-        for kind in (POOL_W, GATE_W, BACK_W):
-            at(l, "S1", z_stage, kind, l, 2)
-        at(l, "S2", z_stage, POOL_W, l, 3)
-        at(l, "S3", z_stage, POOL_W, l, 4)
-        at(l, "S3", z_stage, GATE_W, l, 3)
-        at(l, "S3", z_stage, BACK_W, l, 3)
-        at(l, "S3", z_end, POOL_W, l)
-        at(l, "I", z_stage, GATE_W, l, 4)
-        at(l, "I", z_stage, BACK_W, l, 4)
-        at(l, "P2", z_end, GATE_W, l)
+    at(0, "P1", z_stage, BACK_W, 0, 3)
+    for l in range(layers):
+        if l > 0:
+            for kind in (POOL_W, GATE_W, BACK_W):
+                at(l - 1, "I", z_begin, kind, l)
+            at(l - 1, "P2", z_stage, POOL_W, l, 1, True)
+            at(l, "S0", z_stage, POOL_W, l, 1, False)
+            at(l, "S2", z_stage, POOL_W, l, 2)
+            at(l, "S3", z_end, POOL_W, l)
+            for kind in (GATE_W, BACK_W):
+                at(l, "S0", z_stage, kind, l, 1)
+                at(l, "S1", z_stage, kind, l, 2)
+                at(l, "S3", z_stage, kind, l, 3)
+                at(l, "I", z_stage, kind, l, 4)
+        gate_slot = "P1" if l > 0 else "P2"
+        at(l, gate_slot, z_end, GATE_W, l)
+        at(l, gate_slot, make_gate, l)
         at(l, "P2", z_end, BACK_W, l)
 
     def slot(l, name):
@@ -251,7 +268,7 @@
 
     swap_rows = pl.ds(pl.multiple_of(swap_to[0] * rows_w, rows_w), rows_w)
     swap_who = {"sp": swap_to[0], "tp": swap_to[1]}
-    start(wback_ref.at[0], w_b.at[0, swap_rows], swap_send.at[0], swap_recv.at[0], swap_who)
+    start(wback_ref.at[0], w_b.at[0, swap_rows], swap_recv.at[0], swap_who)
     for c in range(CHUNKS):
         loads[1 + c].wait()
         for way in (0, 1):
@@ -261,7 +278,7 @@
     loads[1 + CHUNKS].wait()
     z_begin(GATE_W, 0)
     rest = pl.ds(1, layers - 1)
-    start(wback_ref.at[rest], w_b.at[rest, swap_rows], swap_send.at[1], swap_recv.at[1], swap_who)
+    start(wback_ref.at[rest], w_b.at[rest, swap_rows], swap_recv.at[1], swap_who)
     loads[2 + CHUNKS].wait()
 
     def pool_term(l, d):
@@ -305,9 +322,10 @@
         sumsq[...] = jnp.zeros_like(sumsq)
         for c in range(CHUNKS):
             prep(l, c, tp)
+        slot(l, "S0")
         x_gather(xs, l, "S", functools.partial(prep, l), None)
 
-        scale = lax.rsqrt(jnp.sum(sumsq[...], axis=1, keepdims=True) * (1.0 / (n_tp * feat)) + EPS)
+        scale = norm_scale()
         if l == 0:
             pool = jnp.dot(xg[...], w_p[l], preferred_element_type=F32)
         else:
@@ -316,17 +334,13 @@
 
         @pl.when(sp > 0)
         def _():
-            start(pin.at[l], halo.at[l, 1], halo_send.at[l, 1], halo_recv.at[l, 1], {"sp": before})
+            start(pin.at[l], halo.at[l, 1], halo_recv.at[l, 1], {"sp": before})
 
         @pl.when(sp < n_sp - 1)
         def _():
-            start(pin.at[l], halo.at[l, 0], halo_send.at[l, 0], halo_recv.at[l, 0], {"sp": after})
-
-        def make_gate():
-            rows_scale = lax.rsqrt(jnp.sum(sumsq[...], axis=1, keepdims=True) * (1.0 / (n_tp * feat)) + EPS)
-            gate_acc = jnp.dot(xg[...], w_g[l], preferred_element_type=F32)
-            gate[...] = jax.nn.sigmoid(gate_acc * rows_scale)
-
+            start(pin.at[l], halo.at[l, 0], halo_recv.at[l, 0], {"sp": after})
+
+        slot(l, "H")
         own_pool = pin[l]
         box = jnp.dot(boxm[1], own_pool, preferred_element_type=F32)
 
@@ -348,8 +362,6 @@
         slot(l, "I")
 
         def finish(c):
-            if c == 0:
-                make_gate()
             branch = None
             for p in range(n_tp):
                 term = lax.dot_general(ps[l, c, (p + half_tp) % n_tp], w_b[l, p * feat:(p + 1) * feat],
@@ -366,36 +378,23 @@
 
         x_gather(ps, l, "P", None, finish)
 
-    arrived(wback_ref.at[0], swap_send.at[0])
-    arrived(wback_ref.at[rest], swap_send.at[1])
-
-    def drained(ref, rows, sem):
-        while rows:
-            now = min(rows, ref.shape[0])
-            arrived(ref.at[pl.ds(0, now)], sem)
-            rows -= now
-
-    sent = {buf_i: sum(reach(way, c) for way in (0, 1) for c in range(CHUNKS)) for buf_i in (0, 1)}
+    arrived(wback_ref, sent)
+    rounds = sum(reach(way, c) for way in (0, 1) for c in range(CHUNKS))
     for l in range(layers):
-        for buf, send in ((xs, x_send), (ps, p_send)):
-            left = sent[0]
-            c = 0
-            while left:
-                now = min(left, n_tp)
-                arrived(buf.at[l, c % CHUNKS, pl.ds(0, now)], send.at[l])
-                left -= now
-                c += 1
-        for kind in range(3):
-            drained(pieces[kind].at[l], (z_reach(0) + z_reach(1)) * rows_w, w_send.at[kind, l])
-            drained(pieces[kind].at[l], n_z * rows_w, peer_send.at[kind, l])
+        for buf in (xs, ps):
+            for c in range(0, rounds, n_tp):
+                arrived(buf.at[l, (c // n_tp) % CHUNKS, pl.ds(0, min(n_tp, rounds - c))], sent)
+        for piece in pieces:
+            arrived(piece.at[l, pl.ds(0, (n_z - 1) * rows_w)], sent)
+            arrived(piece.at[l, pl.ds(0, n_z * rows_w)], sent)
 
         @pl.when(sp > 0)
         def _():
-            arrived(pin.at[l], halo_send.at[l, 1])
+            arrived(pin.at[l], sent)
 
         @pl.when(sp < n_sp - 1)
         def _():
-            arrived(pin.at[l], halo_send.at[l, 0])
+            arrived(pin.at[l], sent)
 
 
 def solution(mesh):
@@ -430,18 +429,13 @@
                 pltpu.VMEM((tokens, 128), F32),
                 pltpu.VMEM(norm_gain.shape, F32),
                 pltpu.VMEM((tokens, chan), F32),
-                dma((layers, 2, half_tp, CHUNKS)),
-                dma((layers, 2, half_tp, CHUNKS)),
-                dma((3, layers, 2, half_z)),
+                dma((2, half_tp, CHUNKS)),
+                dma((2, half_tp, CHUNKS)),
+                dma((3, layers, 4)),
                 dma((layers, 2)),
                 dma((3, layers)),
                 dma((2,)),
-                dma((layers,)),
-                dma((layers,)),
-                dma((3, layers)),
-                dma((3, layers)),
-                dma((layers, 2)),
-                dma((2,)),
+                dma,
                 dma((3 + CHUNKS,)),
             ],
             compiler_params=pltpu.CompilerParams(

time: 147 us -> 143 us (0.973)
  Pallas kernels: 146 us -> 142 us
    pallas_call x1, Pallas kernels: 146 us -> 142 us  [on_device(): pl.pallas_call(functools.partial(mixer, n_sp, n_tp), out_shape=pltpu.VMEM...]
where the time goes in v5:
time: 143 us
  Pallas kernels  142 us (99%)
    pallas_call x1, Pallas kernels, on_device(): pl.pallas_call(functools.partial(mixer, n_sp, n_tp), out_shape=pltpu.VMEM...  142 us

profile of v5, /device:TPU:65, one launch (start us, length us, event | category | flops | bytes accessed | tf_op | source)
XLA Modules:
  0.0 142.8 jit_solution(4386487288645334996)
XLA Ops:
  0.0 142.1 %shard_map.55 = bf16[256,256]{1,0:T(8,128)(2,1)S(1)} custom-call(bf16[256,256]{1,0:T(8,128)(2,1)} %tok_ref.1, f32[3,2048]{1,0:T(4,128)} %gain_in.1, bf16[3,64,128]{2,1,0:T(8,128)(2,1)} %wpool_ref.1, bf16[3,64,256]{2,1,0:T(8,128)(2,1)} %wgate_ref.1, bf16[3,64,128]{2,1,0:T(8,128)(2,1)} %bitcast.1), custom_call_target="tpu_custom_call" | custom-call | tf_op jit(solution)/shard_map/pallas_call | solution.py:412
  142.1 0.7 copy.7

commit v6 on v5

--- a/solution.py
+++ b/solution.py
@@ -14,6 +14,7 @@
 GROUPS = 4
 EPS = 1e-6
 CHUNKS = 4
+POOLED_CHUNKS = 2
 scope = jax.named_scope
 
 RING = {1: 0, 2: 1, 3: 2, 4: 3}
@@ -53,6 +54,7 @@
     chan = wpool_ref.shape[2]
     rows_w = wpool_ref.shape[1]
     ct = tokens // CHUNKS
+    pt = tokens // POOLED_CHUNKS
     half_tp = n_tp // 2
     n_z = n_sp // 2
     half_z = n_z // 2
@@ -101,37 +103,6 @@
     loads.append(pltpu.make_async_copy(gain_in, gain_ref, load_sem.at[2 + CHUNKS]))
     for load in loads:
         load.start()
-
-    with scope("boxes"):
-        window = lax.shift_left(2, (tp * chan) // (n_tp * chan // GROUPS))
-        reach_w = window // 2
-        grid_rows = tokens // GRID_W
-        first = sp * grid_rows
-        total = grid_rows * n_sp
-        ti = lax.broadcasted_iota(jnp.int32, (tokens, tokens), 0)
-        tj = lax.broadcasted_iota(jnp.int32, (tokens, tokens), 1)
-        ri, ci = ti // GRID_W, ti % GRID_W
-        cj = tj % GRID_W
-        col_in = (cj >= ci - reach_w) & (cj < ci + reach_w)
-        for k in range(3):
-            rj = tj // GRID_W + (k - 1) * grid_rows
-            inside = col_in & (rj >= ri - reach_w) & (rj < ri + reach_w)
-            boxm[k] = jnp.where(inside, 1.0, 0.0).astype(BF16)
-        tr = lax.broadcasted_iota(jnp.int32, (tokens, chan), 0)
-        r_at, c_at = tr // GRID_W + first, tr % GRID_W
-        r_n = jnp.minimum(r_at + reach_w, total) - jnp.maximum(r_at - reach_w, 0)
-        c_n = jnp.minimum(c_at + reach_w, GRID_W) - jnp.maximum(c_at - reach_w, 0)
-        inv_count[...] = 1.0 / (r_n * c_n).astype(F32)
-
-        @pl.when(sp == 0)
-        def _():
-            for l in range(layers):
-                halo[l, 0] = jnp.zeros((tokens, chan), BF16)
-
-        @pl.when(sp == n_sp - 1)
-        def _():
-            for l in range(layers):
-                halo[l, 1] = jnp.zeros((tokens, chan), BF16)
 
     with scope("barrier"):
         pl.semaphore_wait(barrier, len(greet))
@@ -209,8 +180,8 @@
     def swap_rest():
         arrived(w_b.at[pl.ds(1, layers - 1), own_rows], swap_recv.at[1], "swap")
 
-    def norm_scale():
-        return lax.rsqrt(jnp.sum(sumsq[...], axis=1, keepdims=True) * (1.0 / (n_tp * feat)) + EPS)
+    def norm_scale(rows=slice(None)):
+        return lax.rsqrt(jnp.sum(sumsq[rows], axis=1, keepdims=True) * (1.0 / (n_tp * feat)) + EPS)
 
     def make_gate(l):
         gate_acc = jnp.dot(xg[...], w_g[l], preferred_element_type=F32)
@@ -281,6 +252,37 @@
     start(wback_ref.at[rest], w_b.at[rest, swap_rows], swap_recv.at[1], swap_who)
     loads[2 + CHUNKS].wait()
 
+    with scope("boxes"):
+        window = lax.shift_left(2, (tp * chan) // (n_tp * chan // GROUPS))
+        reach_w = window // 2
+        grid_rows = tokens // GRID_W
+        first = sp * grid_rows
+        total = grid_rows * n_sp
+        ti = lax.broadcasted_iota(jnp.int32, (tokens, tokens), 0)
+        tj = lax.broadcasted_iota(jnp.int32, (tokens, tokens), 1)
+        ri, ci = ti // GRID_W, ti % GRID_W
+        cj = tj % GRID_W
+        col_in = (cj >= ci - reach_w) & (cj < ci + reach_w)
+        for k in range(3):
+            rj = tj // GRID_W + (k - 1) * grid_rows
+            inside = col_in & (rj >= ri - reach_w) & (rj < ri + reach_w)
+            boxm[k] = jnp.where(inside, 1.0, 0.0).astype(BF16)
+        tr = lax.broadcasted_iota(jnp.int32, (tokens, chan), 0)
+        r_at, c_at = tr // GRID_W + first, tr % GRID_W
+        r_n = jnp.minimum(r_at + reach_w, total) - jnp.maximum(r_at - reach_w, 0)
+        c_n = jnp.minimum(c_at + reach_w, GRID_W) - jnp.maximum(c_at - reach_w, 0)
+        inv_count[...] = 1.0 / (r_n * c_n).astype(F32)
+
+        @pl.when(sp == 0)
+        def _():
+            for l in range(layers):
+                halo[l, 0] = jnp.zeros((tokens, chan), BF16)
+
+        @pl.when(sp == n_sp - 1)
+        def _():
+            for l in range(layers):
+                halo[l, 1] = jnp.zeros((tokens, chan), BF16)
+
     def pool_term(l, d):
         at_d = pl.ds(pl.multiple_of(tp_at(d) * feat, feat), feat)
         return jnp.dot(xg[:, at_d], w_p[l, at_d], preferred_element_type=F32)
@@ -292,12 +294,28 @@
                 total_here = total_here + pool_term(l, d) + pool_term(l, -d)
             pool_acc[...] = total_here
 
+    def send_halo(l, rows):
+        @pl.when(sp > 0)
+        def _():
+            start(pin.at[l, rows], halo.at[l, 1, rows], halo_recv.at[l, 1], {"sp": before})
+
+        @pl.when(sp < n_sp - 1)
+        def _():
+            start(pin.at[l, rows], halo.at[l, 0, rows], halo_recv.at[l, 0], {"sp": after})
+
+    def pool_chunk(l, c):
+        rows = slice(c * ct, (c + 1) * ct)
+        far = pl.ds(pl.multiple_of(tp_at(half_tp) * feat, feat), feat)
+        term = jnp.dot(xg[rows, far], w_p[l, far], preferred_element_type=F32)
+        pin[l, rows] = ((pool_acc[rows] + term) * norm_scale(rows)).astype(BF16)
+        send_halo(l, pl.ds(c * ct, ct))
+
     def x_gather(buf, l, name, each, last):
         deep = stages(x_parts(buf)[0], half_tp)
         for k, ds in enumerate(deep, 1):
             if k == len(deep) and last is None:
                 ahead(l)
-            for c in range(CHUNKS):
+            for c in range(buf.shape[1]):
                 got = []
                 for d in ds:
                     for way in (0, 1):
@@ -308,6 +326,8 @@
                 if each is not None:
                     for d in got:
                         each(c, tp_at(d))
+                if k == len(deep) and last is None and l > 0:
+                    pool_chunk(l, c)
                 if k == len(deep) and last is not None:
                     if c == 0:
                         slot(l, f"{name}{k}")
@@ -325,20 +345,10 @@
         slot(l, "S0")
         x_gather(xs, l, "S", functools.partial(prep, l), None)
 
-        scale = norm_scale()
         if l == 0:
             pool = jnp.dot(xg[...], w_p[l], preferred_element_type=F32)
-        else:
-            pool = pool_acc[...] + pool_term(l, half_tp)
-        pin[l] = (pool * scale).astype(BF16)
-
-        @pl.when(sp > 0)
-        def _():
-            start(pin.at[l], halo.at[l, 1], halo_recv.at[l, 1], {"sp": before})
-
-        @pl.when(sp < n_sp - 1)
-        def _():
-            start(pin.at[l], halo.at[l, 0], halo_recv.at[l, 0], {"sp": after})
+            pin[l] = (pool * norm_scale()).astype(BF16)
+            send_halo(l, pl.ds(0, tokens))
 
         slot(l, "H")
         own_pool = pin[l]
@@ -355,8 +365,8 @@
         box = box + jnp.dot(boxm[0], halo[l, 0], preferred_element_type=F32)
         box = box + jnp.dot(boxm[2], halo[l, 1], preferred_element_type=F32)
         pooled = (box * inv_count[...] - own_pool.astype(F32)).astype(BF16)
-        for c in range(CHUNKS):
-            ps[l, c, tp] = pooled[c * ct:(c + 1) * ct]
+        for c in range(POOLED_CHUNKS):
+            ps[l, c, tp] = pooled[c * pt:(c + 1) * pt]
             for way in (0, 1):
                 x_forward(ps, l, c, 0, way)
         slot(l, "I")
@@ -367,23 +377,25 @@
                 term = lax.dot_general(ps[l, c, (p + half_tp) % n_tp], w_b[l, p * feat:(p + 1) * feat],
                                        (((1,), (1,)), ((), ())), preferred_element_type=F32)
                 branch = term if branch is None else branch + term
-            rows = slice(c * ct, (c + 1) * ct)
-            new = (xs[l, c, tp].astype(F32) + gate[rows] * branch).astype(BF16)
-            if l + 1 < layers:
-                xs[l + 1, c, tp] = new
-                for way in (0, 1):
-                    x_forward(xs, l + 1, c, 0, way)
-            else:
-                out_ref[rows, :] = new
+            for i in range(pt // ct):
+                k = c * (pt // ct) + i
+                rows = slice(k * ct, (k + 1) * ct)
+                new = (xs[l, k, tp].astype(F32) + gate[rows] * branch[i * ct:(i + 1) * ct]).astype(BF16)
+                if l + 1 < layers:
+                    xs[l + 1, k, tp] = new
+                    for way in (0, 1):
+                        x_forward(xs, l + 1, k, 0, way)
+                else:
+                    out_ref[rows, :] = new
 
         x_gather(ps, l, "P", None, finish)
 
     arrived(wback_ref, sent)
-    rounds = sum(reach(way, c) for way in (0, 1) for c in range(CHUNKS))
     for l in range(layers):
         for buf in (xs, ps):
+            rounds = sum(reach(way, c) for way in (0, 1) for c in range(buf.shape[1]))
             for c in range(0, rounds, n_tp):
-                arrived(buf.at[l, (c // n_tp) % CHUNKS, pl.ds(0, min(n_tp, rounds - c))], sent)
+                arrived(buf.at[l, (c // n_tp) % buf.shape[1], pl.ds(0, min(n_tp, rounds - c))], sent)
         for piece in pieces:
             arrived(piece.at[l, pl.ds(0, (n_z - 1) * rows_w)], sent)
             arrived(piece.at[l, pl.ds(0, n_z * rows_w)], sent)
@@ -416,7 +428,7 @@
             out_specs=pl.BlockSpec(memory_space=pltpu.VMEM),
             scratch_shapes=[
                 pltpu.VMEM((layers, CHUNKS, n_tp, ct, feat), BF16),
-                pltpu.VMEM((layers, CHUNKS, n_tp, ct, chan), BF16),
+                pltpu.VMEM((layers, POOLED_CHUNKS, n_tp, tokens // POOLED_CHUNKS, chan), BF16),
                 pltpu.VMEM((tokens, n_tp * feat), BF16),
                 pltpu.VMEM((layers, rows, chan), BF16),
                 pltpu.VMEM((layers, rows, feat), BF16),
@@ -430,7 +442,7 @@
                 pltpu.VMEM(norm_gain.shape, F32),
                 pltpu.VMEM((tokens, chan), F32),
                 dma((2, half_tp, CHUNKS)),
-                dma((2, half_tp, CHUNKS)),
+                dma((2, half_tp, POOLED_CHUNKS)),
                 dma((3, layers, 4)),
                 dma((layers, 2)),
                 dma((3, layers)),

time: 143 us -> 143 us (level)
  no operation moved by 1% of the time
where the time goes in v6:
time: 143 us; the launch traced here: 142 us
  Pallas kernels  142 us (99%)
    pallas_call x1, Pallas kernels, on_device(): pl.pallas_call(functools.partial(mixer, n_sp, n_tp), out_shape=pltpu.VMEM...  142 us

profile of v6, /device:TPU:65, one launch (start us, length us, event | category | flops | bytes accessed | tf_op | source)
XLA Modules:
  0.0 142.4 jit_solution(2233304407152417641)
XLA Ops:
  0.0 141.8 %shard_map.55 = bf16[256,256]{1,0:T(8,128)(2,1)S(1)} custom-call(bf16[256,256]{1,0:T(8,128)(2,1)} %tok_ref.1, f32[3,2048]{1,0:T(4,128)} %gain_in.1, bf16[3,64,128]{2,1,0:T(8,128)(2,1)} %wpool_ref.1, bf16[3,64,256]{2,1,0:T(8,128)(2,1)} %wgate_ref.1, bf16[3,64,128]{2,1,0:T(8,128)(2,1)} %bitcast.1), custom_call_target="tpu_custom_call" | custom-call | tf_op jit(solution)/shard_map/pallas_call | solution.py:424
  141.8 0.7 copy.7

commit v7 on v6

--- a/solution.py
+++ b/solution.py
@@ -192,8 +192,8 @@
     def at(l, slot, *action):
         plan.setdefault((l, slot), []).append(action)
 
-    at(0, "S1", z_stage, POOL_W, 0, 1, True)
-    at(0, "S2", z_stage, GATE_W, 0, 1)
+    at(0, "S2", z_stage, POOL_W, 0, 1, True)
+    at(0, "S3", z_stage, GATE_W, 0, 1)
     at(0, "S2", back_begin)
     at(0, "S3", z_stage, POOL_W, 0, 1, False)
     at(0, "S4", z_stage, POOL_W, 0, 2)

time: 143 us -> 142 us (level)
  no operation moved by 1% of the time
where the time goes in v7:
time: 142 us
  Pallas kernels  142 us (100%)
    pallas_call x1, Pallas kernels, on_device(): pl.pallas_call(functools.partial(mixer, n_sp, n_tp), out_shape=pltpu.VMEM...  142 us

profile of v7, /device:TPU:65, one launch (start us, length us, event | category | flops | bytes accessed | tf_op | source)
XLA Modules:
  0.0 142.3 jit_solution(16463130346140550968)
XLA Ops:
  0.0 141.6 %shard_map.55 = bf16[256,256]{1,0:T(8,128)(2,1)S(1)} custom-call(bf16[256,256]{1,0:T(8,128)(2,1)} %tok_ref.1, f32[3,2048]{1,0:T(4,128)} %gain_in.1, bf16[3,64,128]{2,1,0:T(8,128)(2,1)} %wpool_ref.1, bf16[3,64,256]{2,1,0:T(8,128)(2,1)} %wgate_ref.1, bf16[3,64,128]{2,1,0:T(8,128)(2,1)} %bitcast.1), custom_call_target="tpu_custom_call" | custom-call | tf_op jit(solution)/shard_map/pallas_call | solution.py:424
  141.6 0.7 copy.7
